TPU v7x, 32 devices: a whole 2x2x4 slice. The times are simulated.
32 devices in a mesh: ep: 4 (over y, x), tp: 8 (over z, core).
Axes of the slice: x: 2, y: 2, z: 4, core: 2. Of those that a mesh axis runs over, the one named last changes fastest.
Arguments:
- tokens: bfloat16 [2048, 2048], P('ep', 'tp'), may hold values from -6 to 6
- norm_gain: float32 [2048], replicated, may hold values from 0.1 to 1.9
- norm_shift: float32 [2048], replicated, may hold values from -3 to 3
- expert_ids: int32 [2048, 6], P('ep'), may hold values from 0 to 31, all different within a row; in each aligned block of 64 rows (0 to 63, 64 to 127, ...) at most 24 rows name the same one
- affinity: float32 [2048, 6], P('ep'), may hold values from 0.05 to 1
- expert_gate: bfloat16 [32, 2048, 512], P(('ep', 'tp')), may hold values from -0.125 to 0.125
- expert_up: bfloat16 [32, 2048, 512], P(('ep', 'tp')), may hold values from -0.125 to 0.125
- expert_down: bfloat16 [32, 512, 2048], P(('ep', 'tp')), may hold values from -0.25 to 0.25
- shared_gate: bfloat16 [512, 2048], P('tp'), may hold values from -0.125 to 0.125
- shared_up: bfloat16 [512, 2048], P('tp'), may hold values from -0.125 to 0.125
- shared_down: bfloat16 [512, 2048], replicated, may hold values from -0.25 to 0.25
Outputs:
- mixed: bfloat16 [2048, 2048], P(('ep', 'tp'))
Inputs may be any that keep to these rules, and one draw needn't show every extreme that they name: `expert_ids`: each row names 6 different experts; in each aligned block of 64 rows (the rows of one device of tp) no expert is named more than 24 times, and in some blocks an expert is named exactly 24 times.
All inputs are finite; a program needn't handle non-finite values.
Results may differ from a plain program's by a relative error of at most 0.0069.
Values may be sent and summed in bfloat16 or wider, within the bound.
No kernel may reach another device: no remote copies, remote signals or barrier semaphores. Data moves between devices by JAX's collectives and lax.ppermute only.
A program may use at most 64 MiB of HBM per device.

v0:
```python
import jax
import jax.numpy as jnp
from jax import lax
from jax.sharding import PartitionSpec as P

ROUTED_SCALE = 2.5
EPSILON = 1e-05


def pair_ranks(flat_ids, expert_count):
    onehot = flat_ids[..., None] == jnp.arange(expert_count, dtype=jnp.int32)
    running = jnp.cumsum(onehot.astype(jnp.int32), axis=-2)
    return jnp.sum(jnp.where(onehot, running, 0), axis=-1) - 1


def expert_rows(tok_rows, w_gate, w_up, w_down):
    gate_act = jnp.dot(tok_rows, w_gate, preferred_element_type=jnp.float32)
    up_act = jnp.dot(tok_rows, w_up, preferred_element_type=jnp.float32)
    hidden = (jax.nn.silu(gate_act) * up_act).astype(jnp.bfloat16)
    return jnp.dot(hidden, w_down, preferred_element_type=jnp.float32).astype(jnp.bfloat16)


def weighted_sum(source_rows, slot_index, pair_weight, top_count):
    total = jnp.zeros((slot_index.shape[0], source_rows.shape[1]), jnp.float32)
    for column in range(top_count):
        picked = jnp.take(source_rows, slot_index[:, column], axis=0, mode="fill", fill_value=0)
        total = total + pair_weight[:, column : column + 1] * picked.astype(jnp.float32)
    return total


def on_device(
    tokens,
    norm_gain,
    norm_shift,
    expert_ids,
    affinity,
    expert_gate,
    expert_up,
    expert_down,
    shared_gate,
    shared_up,
    shared_down,
):
    ep_count = lax.axis_size("ep")
    tp_count = lax.axis_size("tp")
    tp_index = lax.axis_index("tp")
    whole = lax.all_gather(tokens, "tp", axis=1, tiled=True)
    tok_count = whole.shape[0]
    width = whole.shape[1]
    top_count = expert_ids.shape[1]
    block_rows = tok_count // tp_count
    expert_count = ep_count * tp_count
    slot_cap = max(1, 2 * block_rows * top_count // expert_count)
    slot_total = expert_count * slot_cap
    values = whole.astype(jnp.float32)
    center = values - jnp.mean(values, axis=1, keepdims=True)
    spread = jnp.mean(center * center, axis=1, keepdims=True)
    normed = (center * lax.rsqrt(spread + EPSILON) * norm_gain + norm_shift).astype(jnp.bfloat16)
    weights = affinity / jnp.sum(affinity, axis=1, keepdims=True) * ROUTED_SCALE
    contract = (((1,), (1,)), ((), ()))
    shared_g = lax.dot_general(shared_gate, normed, contract, preferred_element_type=jnp.float32)
    shared_u = lax.dot_general(shared_up, normed, contract, preferred_element_type=jnp.float32)
    shared_hidden = (jax.nn.silu(shared_g) * shared_u).astype(jnp.bfloat16)
    own_hidden = lax.all_to_all(shared_hidden, "tp", split_axis=1, concat_axis=0, tiled=True)
    shared_out = lax.dot_general(
        own_hidden, shared_down, (((0,), (0,)), ((), ())), preferred_element_type=jnp.float32
    )
    block_ids = expert_ids.reshape(tp_count, block_rows * top_count)
    ranks = pair_ranks(block_ids, expert_count)
    group_index = block_ids // tp_count
    mine = block_ids % tp_count == tp_index
    block_index = jnp.arange(tp_count, dtype=jnp.int32)[:, None]
    dest = jnp.where(mine, (group_index * tp_count + block_index) * slot_cap + ranks, slot_total)
    token_index = (
        block_index * block_rows
        + jnp.arange(block_rows * top_count, dtype=jnp.int32)[None, :] // top_count
    )
    source_row = (
        jnp.full((slot_total + 1,), tok_count, jnp.int32)
        .at[dest.reshape(-1)]
        .set(token_index.reshape(-1))[:slot_total]
    )
    outgoing = jnp.take(normed, source_row, axis=0, mode="fill", fill_value=0).reshape(
        ep_count, tp_count, slot_cap, width
    )
    incoming = lax.all_to_all(outgoing, "ep", split_axis=0, concat_axis=0, tiled=True)
    result = expert_rows(incoming.reshape(-1, width), expert_gate[0], expert_up[0], expert_down[0])
    returned = lax.all_to_all(
        result.reshape(incoming.shape), "ep", split_axis=0, concat_axis=0, tiled=True
    )
    pair_slot = dest.reshape(tok_count, top_count)
    back_rows = returned.reshape(slot_total, width)
    routed = lax.psum_scatter(
        weighted_sum(back_rows, pair_slot, weights, top_count),
        "tp",
        scatter_dimension=0,
        tiled=True,
    )
    return (routed + shared_out).astype(jnp.bfloat16)


def solution(mesh):
    placed = (
        P("ep", "tp"),
        P(),
        P(),
        P("ep", None),
        P("ep", None),
        P(("ep", "tp"), None, None),
        P(("ep", "tp"), None, None),
        P(("ep", "tp"), None, None),
        P("tp", None),
        P("tp", None),
        P(),
    )
    return jax.shard_map(
        on_device, mesh=mesh, in_specs=placed, out_specs=P(("ep", "tp"), None), check_vma=False
    )
```

profile of v0, /device:TPU:0, one launch (start us, length us, event | category | flops | bytes accessed | tf_op | source)
XLA Modules:
  0.0 271.8 jit_solution(16597467197731617035)
XLA Ops:
  6.5 0.7 all-gather.2.cloned.1.call-update
  7.3 0.9 copy.34
  8.1 0.2 eq.48
  8.3 0.2 reshape.242
  8.5 0.2 eq.52
  8.8 6.9 %reduce-window.6 = s32[8,32,3,128]{3,1,2,0:T(8,128)S(1)} reduce-window(s32[8,32,3,128]{3,1,2,0:T(8,128)S(1)} %fusion.20, s32[]{:T(128)} %constant.82.clone.1), window={size=1x1x1x128 pad=0_0x0_0x0_0x127_0}, to_apply=%region_1.0 | reduce-window | flops 12484608 | bytes 786436 | tf_op jit(solution)/shard_map/reduce-window
  15.8 0.2 slice.78
  15.9 0.2 copy.40
  16.1 0.1 fusion.29
  16.3 0.2 fusion.19
  16.5 0.1 compare_select_fusion
  16.6 11.8 %scatter_custom_fusion = s32[769]{0:T(1024)S(1)} fusion(s32[3072]{0:T(1024)S(1)} %bitcast.82, s32[3072]{0:T(1024)S(1)} %reshape.307, s32[]{:T(128)} %constant.81.clone.1), kind=kCustom, calls=%fused_computation.94 | custom fusion | bytes 3080 | tf_op jit(solution)/shard_map/scatter | solution.py:81
  28.4 0.1 slice.51
  28.5 13.8 %all-gather.2.cloned.1.call-done = bf16[512,2048]{1,0:T(8,128)(2,1)} async-done(((bf16[512,256]{1,0:T(8,128)(2,1)}), bf16[512,2048]{1,0:T(8,128)(2,1)}) %all-gather.2.cloned.1.call-update) | async-done | bytes 2097168 | tf_op jit(solution)/shard_map/all_gather | solution.py:47
  42.3 2.1 convert_reduce_fusion
  44.4 0.1 copy-done.2
  44.5 0.7 fusion.2
  45.2 2.2 fusion.5
  47.4 9.0 %gather_fusion = bf16[768,2048]{1,0:T(8,128)(2,1)} fusion(bf16[512,2048]{1,0:T(8,128)(2,1)} %fusion.5, s32[1024]{0:T(1024)S(1)} %pad_clamp_fusion.6), kind=kCustom, calls=%fused_computation.6 | custom fusion | bytes 6294528 | tf_op jit(solution)/shard_map/jit(_take)/gather | solution.py:83
  56.4 3.9 %broadcast_select_fusion = bf16[4,8,24,2048]{3,2,1,0:T(8,128)(2,1)} fusion(bf16[4,8,24,2048]{3,2,1,0:T(8,128)(2,1)} %bitcast.77, pred[4,8,24]{2,1,0:T(8,128)(4,1)S(1)} %compare_and_fusion), kind=kLoop, calls=%fused_computation.18 | loop fusion | flops 1572864 | bytes 6292224 | tf_op jit(solution)/shard_map/jit(_take)/select_n | solution.py:83
  60.3 4.9 %all-to-all-start = ((bf16[4,8,24,2048]{3,2,1,0:T(8,128)(2,1)}), bf16[4,8,24,2048]{3,2,1,0:T(8,128)(2,1)}, u32[]{:S(2)}, u32[]{:S(2)}) async-start(bf16[4,8,24,2048]{3,2,1,0:T(8,128)(2,1)} %broadcast_select_fusion), calls=%async_computation | async-start | bytes 6291456 | tf_op jit(solution)/shard_map/all_to_all | solution.py:86
  65.2 0.1 add.204
  65.3 0.2 sub.37
  65.5 0.3 fusion.26
  65.8 0.8 slice_reduce_fusion.5
  66.7 35.2 %all-to-all-done = bf16[4,8,24,2048]{3,2,1,0:T(8,128)(2,1)} async-done(((bf16[4,8,24,2048]{3,2,1,0:T(8,128)(2,1)}), bf16[4,8,24,2048]{3,2,1,0:T(8,128)(2,1)}, u32[]{:S(2)}, u32[]{:S(2)}) %all-to-all-start) | async-done | bytes 3145760 | tf_op jit(solution)/shard_map/all_to_all | solution.py:86
  101.9 5.6 %fusion.10 = f32[768,512]{1,0:T(8,128)} fusion(bf16[768,2048]{1,0:T(8,128)(2,1)} %bitcast.5, bf16[1,2048,512]{2,1,0:T(8,128)(2,1)} %param.18), kind=kOutput, calls=%fused_computation.24 | convolution fusion | flops 1610612736 | bytes 6815744 | tf_op jit(solution)/shard_map/dot_general | solution.py:17
  107.4 8.2 %convolution_convert_fusion = bf16[768,2048]{1,0:T(8,128)(2,1)} fusion(bf16[1,512,2048]{2,1,0:T(8,128)(2,1)S(1)} %copy-done, f32[768,512]{1,0:T(8,128)} %fusion.10, bf16[768,2048]{1,0:T(8,128)(2,1)} %bitcast.5, bf16[1,2048,512]{2,1,0:T(8,128)(2,1)} %param.19), kind=kOutput, calls=%fused_computation.17 | convolution fusion | flops 3225157632 | bytes 12058624 | tf_op jit(solution)/shard_map/dot_general | solution.py:20
  115.6 4.6 %all-to-all-start.1 = ((bf16[4,8,24,2048]{3,2,1,0:T(8,128)(2,1)}), bf16[4,8,24,2048]{3,2,1,0:T(8,128)(2,1)}, u32[]{:S(2)}, u32[]{:S(2)}) async-start(bf16[4,8,24,2048]{3,2,1,0:T(8,128)(2,1)} %bitcast.78), calls=%async_computation.1 | async-start | bytes 6291456 | tf_op jit(solution)/shard_map/all_to_all | solution.py:88
  120.5 35.7 %all-to-all-done.1 = bf16[4,8,24,2048]{3,2,1,0:T(8,128)(2,1)} async-done(((bf16[4,8,24,2048]{3,2,1,0:T(8,128)(2,1)}), bf16[4,8,24,2048]{3,2,1,0:T(8,128)(2,1)}, u32[]{:S(2)}, u32[]{:S(2)}) %all-to-all-start.1) | async-done | bytes 3145760 | tf_op jit(solution)/shard_map/all_to_all | solution.py:88
  156.2 7.8 %gather_fusion.6 = bf16[512,2048]{1,0:T(8,128)(2,1)} fusion(bf16[768,2048]{1,0:T(8,128)(2,1)} %bitcast.10, s32[1024]{0:T(1024)S(1)} %pad_clamp_fusion), kind=kCustom, calls=%fused_computation.5.clone | custom fusion | bytes 4196352 | tf_op jit(solution)/shard_map/jit(_take)/gather | solution.py:26
  164.0 7.5 %gather_fusion.5 = bf16[512,2048]{1,0:T(8,128)(2,1)} fusion(bf16[768,2048]{1,0:T(8,128)(2,1)} %bitcast.10, s32[1024]{0:T(1024)S(1)} %pad_clamp_fusion.1), kind=kCustom, calls=%fused_computation.4.clone | custom fusion | bytes 4196352 | tf_op jit(solution)/shard_map/jit(_take)/gather | solution.py:26
  171.6 7.5 %gather_fusion.4 = bf16[512,2048]{1,0:T(8,128)(2,1)} fusion(bf16[768,2048]{1,0:T(8,128)(2,1)} %bitcast.10, s32[1024]{0:T(1024)S(1)} %pad_clamp_fusion.2), kind=kCustom, calls=%fused_computation.3.clone | custom fusion | bytes 4196352 | tf_op jit(solution)/shard_map/jit(_take)/gather | solution.py:26
  179.1 7.5 %gather_fusion.3 = bf16[512,2048]{1,0:T(8,128)(2,1)} fusion(bf16[768,2048]{1,0:T(8,128)(2,1)} %bitcast.10, s32[1024]{0:T(1024)S(1)} %pad_clamp_fusion.3), kind=kCustom, calls=%fused_computation.2.clone | custom fusion | bytes 4196352 | tf_op jit(solution)/shard_map/jit(_take)/gather | solution.py:26
  186.6 7.5 %gather_fusion.2 = bf16[512,2048]{1,0:T(8,128)(2,1)} fusion(bf16[768,2048]{1,0:T(8,128)(2,1)} %bitcast.10, s32[1024]{0:T(1024)S(1)} %pad_clamp_fusion.4), kind=kCustom, calls=%fused_computation.1.clone | custom fusion | bytes 4196352 | tf_op jit(solution)/shard_map/jit(_take)/gather | solution.py:26
  194.1 7.8 %gather_fusion.1 = bf16[512,2048]{1,0:T(8,128)(2,1)} fusion(bf16[768,2048]{1,0:T(8,128)(2,1)} %bitcast.10, s32[1024]{0:T(1024)S(1)} %pad_clamp_fusion.5), kind=kCustom, calls=%fused_computation.clone | custom fusion | bytes 4196352 | tf_op jit(solution)/shard_map/jit(_take)/gather | solution.py:26
  202.0 9.0 %multiply_add_fusion = f32[512,2048]{1,0:T(8,128)} fusion(bf16[512,2048]{1,0:T(8,128)(2,1)} %gather_fusion.6, bf16[512,2048]{1,0:T(8,128)(2,1)} %gather_fusion.5, bf16[512,2048]{1,0:T(8,128)(2,1)} %gather_fusion.4, bf16[512,2048]{1,0:T(8,128)(2,1)} %gather_fusion.3, bf16[512,2048]{1,0:T(8,128)(2,1)} %gather_fusion.2, bf16[512,2048]{1,0:T(8,128)(2,1)} %gather_fusion.1, ...), kind=kLoop, calls=%fused_computation.16 | loop fusion | flops 24117248 | bytes 16792576 | tf_op jit(solution)/shard_map/add | solution.py:27
  211.1 0.9 copy-done.3
  212.0 2.5 convolution_bitcast_fusion.1
  214.5 0.8 fusion.15
  215.3 0.1 copy.46
  215.4 0.2 reshape.338
  215.6 11.3 %all_to_all.29 = bf16[8,2,2048]{2,1,0:T(2,128)(2,1)S(1)} all-to-all(bf16[8,2,2048]{2,1,0:T(2,128)(2,1)S(1)} %reshape.338), channel_id=1, replica_groups=mesh['ep'=4,'tp'=8] {'tp'}, dimensions={0} | all-to-all | bytes 131072 | tf_op jit(solution)/shard_map/all_to_all | solution.py:64
  226.9 0.1 reshape.339
  227.0 0.1 copy.45
  227.1 0.1 all_to_all.25
  227.3 34.9 %reduce-scatter.2.cloned.1.call-done = f32[64,2048]{1,0:T(8,128)} async-done(((f32[512,2048]{1,0:T(8,128)}), f32[64,2048]{1,0:T(8,128)}) %reduce-scatter.2.cloned.1.call-update) | async-done | bytes 524304 | tf_op jit(solution)/shard_map/reduce_scatter | solution.py:93
  262.1 2.9 %fusion.6 = bf16[64,2048]{1,0:T(8,128)(2,1)} fusion(f32[64,2048]{1,0:T(8,128)} %reduce-scatter.2.cloned.1.call-done, bf16[512,64]{0,1:T(8,128)(2,1)S(1)} %all_to_all.25, bf16[512,2048]{1,0:T(8,128)(2,1)} %param.23), kind=kOutput, calls=%fused_computation.20 | convolution fusion | flops 134479872 | bytes 2949120 | tf_op jit(solution)/shard_map/dot_general | solution.py:65
  (50 shorter events, 0.4 us)
Async XLA Ops:
  6.5 100.9 %copy-start = (bf16[1,512,2048]{2,1,0:T(8,128)(2,1)S(1)}, bf16[1,512,2048]{2,1,0:T(8,128)(2,1)}, u32[]{:S(2)}) copy-start(bf16[1,512,2048]{2,1,0:T(8,128)(2,1)} %param.20) | copy-start | bytes 6291460
  6.5 35.8 %all-gather.2.cloned.1.call-start = ((), (), s32[]{:S(2)}) async-start(), calls=%async_computation.4 | async-start | bytes 2359296 | tf_op jit(solution)/shard_map/all_gather | solution.py:47
  42.3 2.2 copy-start.2
  42.3 2.9 %copy-start.5 = (f32[2048]{0:T(1024)S(1)}, f32[2048]{0:T(1024)}, u32[]{:S(2)}) copy-start(f32[2048]{0:T(1024)} %param.15) | copy-start | bytes 24580
  42.3 2.9 %copy-start.6 = (f32[2048]{0:T(1024)S(1)}, f32[2048]{0:T(1024)}, u32[]{:S(2)}) copy-start(f32[2048]{0:T(1024)} %param.14) | copy-start | bytes 24580
  60.3 5.3 %copy-start.4 = (f32[512,6]{0,1:T(8,128)S(1)}, f32[512,6]{0,1:T(8,128)}, u32[]{:S(2)}) copy-start(f32[512,6]{0,1:T(8,128)} %param.17) | copy-start | bytes 36868
  60.3 41.6 %all-to-all-start = ((bf16[4,8,24,2048]{3,2,1,0:T(8,128)(2,1)}), bf16[4,8,24,2048]{3,2,1,0:T(8,128)(2,1)}, u32[]{:S(2)}, u32[]{:S(2)}) async-start(bf16[4,8,24,2048]{3,2,1,0:T(8,128)(2,1)} %broadcast_select_fusion), calls=%async_computation | async-start | bytes 6291456 | tf_op jit(solution)/shard_map/all_to_all | solution.py:86
  115.6 40.6 %all-to-all-start.1 = ((bf16[4,8,24,2048]{3,2,1,0:T(8,128)(2,1)}), bf16[4,8,24,2048]{3,2,1,0:T(8,128)(2,1)}, u32[]{:S(2)}, u32[]{:S(2)}) async-start(bf16[4,8,24,2048]{3,2,1,0:T(8,128)(2,1)} %bitcast.78), calls=%async_computation.1 | async-start | bytes 6291456 | tf_op jit(solution)/shard_map/all_to_all | solution.py:88
  120.3 141.9 %reduce-scatter.2.cloned.1.call-start = ((), (), s32[]{:S(2)}) async-start(), calls=%async_computation.5 | async-start | bytes 4718592 | tf_op jit(solution)/shard_map/reduce_scatter | solution.py:93
  211.0 0.9 copy-start.3
  212.0 2.5 copy-start.1
  212.0 2.5 copy-start.7
Sparse Core Ops, SparseCore 0:
  8.9 33.3 all-gather.1
  211.2 50.8 reduce-scatter.1
where the time goes:
time: 273 us; the launch traced here: 272 us
  waiting for transfers between devices  120 us (44%)
  local copies, waits for them, and re-layouts  71.2 us (26%)
  other arithmetic  25.8 us (9%)
  matrix products  19.9 us (7%)
  between operations  13.8 us (5%)
  blocking collectives  11.3 us (4%)
  starting transfers between devices  9.63 us (4%)
    gather x6, local copies, waits for them, and re-layouts, weighted_sum(): jnp.take(source_rows, slot_index[:, column], axis=0, mode='fill', fill_va...  45.7 us
    all_to_all x1, waiting for transfers between devices, on_device(): lax.all_to_all(result.reshape(incoming.shape), 'ep', split_axis=0, concat...  35.7 us
    all_to_all x1, waiting for transfers between devices, on_device(): lax.all_to_all(outgoing, 'ep', split_axis=0, concat_axis=0, tiled=True)  35.2 us
    reduce_scatter x1, waiting for transfers between devices, on_device(): lax.psum_scatter(weighted_sum(back_rows, pair_slot, weights, top_count),...  34.9 us
    all_gather x1, waiting for transfers between devices, on_device(): whole = lax.all_gather(tokens, 'tp', axis=1, tiled=True)  13.8 us
    scatter x1, local copies, waits for them, and re-layouts, on_device(): source_row = jnp.full((slot_total + 1,), tok_count, jnp.int32).at[dest.re...  11.8 us
    all_to_all x1, blocking collectives, on_device(): lax.all_to_all(shared_hidden, 'tp', split_axis=1, concat_axis=0, tiled=True)  11.3 us
    add x1, other arithmetic, weighted_sum(): total + pair_weight[:, column:column + 1] * picked.astype(jnp.float32)  9.05 us
  transfers between devices with their start and end apart: 4, of which 4 were waited for; matrix products, arithmetic and copies ran while one was open for 10% of the time, Pallas kernels for 0%

commit v1 on v0

v1 whole, which is shorter than its diff:
```python
import functools

import jax
import jax.numpy as jnp
from jax import lax
from jax.experimental import pallas as pl
from jax.experimental.pallas import tpu as pltpu
from jax.sharding import PartitionSpec as P


ROUTED_SCALE = 2.5
EPSILON = 1e-05


F32 = jnp.float32
BF16 = jnp.bfloat16
VM = pl.BlockSpec(memory_space=pltpu.VMEM)
MIB = 1 << 20


def call(body, outs, operands, limit=16, scratch=(), specs=None):
    return pl.pallas_call(
        body,
        out_shape=outs,
        in_specs=specs or [VM] * len(operands),
        out_specs=jax.tree.map(lambda _: VM, outs),
        scratch_shapes=list(scratch),
        compiler_params=pltpu.CompilerParams(vmem_limit_bytes=limit * MIB),
    )(*operands)


def silu_times(gate, up):
    return (gate / (1.0 + jnp.exp(-gate)) * up).astype(BF16)


def route_body(block, cap, chunks, ids, aff, *rest):
    outs = rest[4:-4]
    for source, target in zip(rest[:4], rest[-4:]):
        target[...] = source[...]
    hosts, levels = lax.axis_size("ep"), lax.axis_size("tp") // 2
    members = 2 * levels
    group, column = lax.axis_index("ep"), lax.axis_index("tp")
    core = lax.rem(column, 2)
    count = ids.shape[1]
    row = lax.broadcasted_iota(jnp.int32, (count, count), 0)
    col = lax.broadcasted_iota(jnp.int32, (count, count), 1)
    upper = jnp.where((row // block == col // block) & (row < col), 1.0, 0.0).astype(BF16)
    here = ids[...]
    share = aff[...]
    share = share / jnp.sum(share, axis=0, keepdims=True) * ROUTED_SCALE
    marks, picked = [], []
    for s in range(2):
        for k in range(hosts):
            hit = here == (group ^ k) * members + (column ^ s)
            marks.append(jnp.max(jnp.where(hit, 1.0, 0.0), axis=0, keepdims=True))
            picked.append(jnp.sum(jnp.where(hit, share, 0.0), axis=0, keepdims=True))
    mark = jnp.concatenate(marks, axis=0)
    weight = jnp.concatenate(picked, axis=0)
    rank = jnp.dot(mark.astype(BF16), upper, preferred_element_type=F32).astype(jnp.int32)
    rank = jnp.where(mark > 0, rank, -count)
    for q, chunk in enumerate(chunks):
        key, key_own, weight_own = outs[3 * q : 3 * q + 3]
        half = len(chunk) * block

        def arranged(array, side):
            starts = [(2 * a + side) * block for a in chunk]
            return jnp.concatenate([array[:, n : n + block] for n in starts], axis=1)

        ranks = [arranged(rank, side) for side in range(2)]
        place = lax.broadcasted_iota(jnp.int32, ranks[0].shape, 1) // block * cap
        ranks = [r + place for r in ranks]
        for side in range(2):
            key[:, side * half : (side + 1) * half] = (
                ranks[side][:hosts] + side * len(chunk) * cap * jnp.where(ranks[side][:hosts] >= 0, 1, 0)
            )
        key_own[...] = jnp.where(core == 0, ranks[0], ranks[1])
        weight_own[...] = jnp.where(core == 0, arranged(weight, 0), arranged(weight, 1))


def norm_body(hosts, *refs):
    levels = lax.axis_size("tp") // 2
    column = lax.axis_index("tp")
    level, core = column // 2, lax.rem(column, 2)
    pieces = 2 * levels
    parts = refs[:pieces]
    gain, shift, key, gate_own, up_own, gate_other, up_other = refs[pieces : pieces + 7]
    slots = refs[pieces + 7 : pieces + 7 + hosts]
    hidden = refs[pieces + 7 + hosts]
    rows, width = parts[0].shape
    cap = slots[0].shape[1]
    scale = 1.0 / (pieces * width)
    mean = sum(jnp.sum(p[...].astype(F32), axis=1, keepdims=True) for p in parts) * scale
    spread = 0.0
    for p in parts:
        center = p[...].astype(F32) - mean
        spread = spread + jnp.sum(center * center, axis=1, keepdims=True)
    factor = lax.rsqrt(spread * scale + EPSILON)
    order = lax.broadcasted_iota(jnp.int32, (cap, rows), 0)
    pick = jnp.concatenate(
        [jnp.where(order == key[k : k + 1, :], 1.0, 0.0) for k in range(hosts)], axis=0
    ).astype(BF16)
    half = rows // 2
    contract = (((1,), (1,)), ((), ()))
    acts = [0.0] * 4
    for n, p in enumerate(parts):
        at = 2 * (level ^ (n // 2)) + (core ^ (n % 2))
        span = pl.ds(pl.multiple_of(at * width, width), width)
        normed = (p[...].astype(F32) - mean) * factor * gain[:, span] + shift[:, span]
        normed = normed.astype(BF16)
        moved = jnp.dot(pick, normed, preferred_element_type=F32).astype(BF16)
        for k in range(hosts):
            slots[k][at] = moved[k * cap : (k + 1) * cap]
        owned = jnp.where(core == 0, normed[:half], normed[half:])
        for i, w in enumerate((gate_own, gate_other, up_own, up_other)):
            acts[i] = acts[i] + lax.dot_general(
                owned, w[:, span], contract, preferred_element_type=F32
            )
    gate = jnp.concatenate(acts[:2], axis=1)
    up = jnp.concatenate(acts[2:], axis=1)
    hidden[...] = silu_times(gate, up)


def expert_body(hosts, *refs):
    core = lax.rem(lax.axis_index("tp"), 2)
    sources = refs[:hosts]
    w_gate, w_up, w_down = refs[hosts : hosts + 3]
    outs = refs[hosts + 3 : 3 * hosts + 3]
    rows, near_down, arrived = refs[3 * hosts + 3 :]
    fetch = pltpu.make_async_copy(w_down.at[0], near_down, arrived)
    fetch.start()
    pieces, cap, width = sources[0].shape
    for k in range(hosts):
        for n in range(pieces):
            rows[k * cap : (k + 1) * cap, n * width : (n + 1) * width] = sources[k][n]
    gate = jnp.dot(rows[...], w_gate[0], preferred_element_type=F32)
    up = jnp.dot(rows[...], w_up[0], preferred_element_type=F32)
    hidden = silu_times(gate, up)
    fetch.wait()
    result = jnp.dot(hidden, near_down[...], preferred_element_type=F32).astype(BF16)
    half = cap // 2
    for k in range(hosts):
        low = result[k * cap : k * cap + half]
        high = result[k * cap + half : (k + 1) * cap]
        outs[k][...] = jnp.where(core == 0, low, high)
        outs[hosts + k][...] = jnp.where(core == 0, high, low)


def combine_body(chunk, *refs):
    hosts, levels = lax.axis_size("ep"), lax.axis_size("tp") // 2
    column = lax.axis_index("tp")
    level = column // 2
    returned = refs[: 2 * hosts]
    key, weight, hidden, down = refs[2 * hosts : 2 * hosts + 4]
    outs = refs[2 * hosts + 4 : 2 * hosts + 4 + levels]
    whole = refs[2 * hosts + 4 + levels]
    cap = returned[0].shape[0]
    count = key.shape[1]
    block = outs[0].shape[0]
    order = lax.broadcasted_iota(jnp.int32, (cap, count), 0)
    mix = jnp.concatenate(
        [
            jnp.where(order == key[n : n + 1, :], weight[n : n + 1, :], 0.0)
            for n in range(2 * hosts)
        ],
        axis=0,
    ).astype(BF16)
    source = jnp.concatenate([r[...] for r in returned], axis=0)
    units = hidden.shape[1] // 2
    near = down[pl.ds(pl.multiple_of(column * units, units), units), :]
    far = down[pl.ds(pl.multiple_of((column ^ 1) * units, units), units), :]
    whole[...] = lax.dot_general(
        mix, source, (((0,), (0,)), ((), ())), preferred_element_type=F32
    ) + jnp.dot(hidden[...], jnp.concatenate([near, far], axis=0), preferred_element_type=F32)
    for k in range(levels):
        spot = sum(jnp.where((level ^ k) == a, n, 0) for n, a in enumerate(chunk))
        part = whole[pl.ds(pl.multiple_of(spot * block, block), block), :]
        outs[k][...] = part.astype(outs[k].dtype)


def final_body(chunks, *refs):
    levels = lax.axis_size("tp") // 2
    level = lax.axis_index("tp") // 2
    out = refs[-1]
    for q, chunk in enumerate(chunks):
        parts = refs[q * levels : (q + 1) * levels]
        inside = functools.reduce(jnp.logical_or, [level == a for a in chunk])

        @pl.when(inside)
        def _():
            out[...] = sum(p[...].astype(F32) for p in parts).astype(BF16)


def on_device(
    tokens,
    norm_gain,
    norm_shift,
    expert_ids,
    affinity,
    expert_gate,
    expert_up,
    expert_down,
    shared_gate,
    shared_up,
    shared_down,
):
    hosts = lax.axis_size("ep")
    members = lax.axis_size("tp")
    levels = members // 2
    count, width = tokens.shape
    top = expert_ids.shape[1]
    full = width * members
    block = count // members
    cap = max(1, 2 * block * top // (hosts * members))
    units = shared_gate.shape[0]

    if levels % 4 == 0:
        edge = levels // 4
        inner = list(range(edge, levels - edge))
        chunks = [[a for a in range(levels) if a not in inner], inner]
    else:
        chunks = [list(range(levels))]
    per = len(chunks[0])
    rows = 2 * per * block
    shape = jax.ShapeDtypeStruct

    def along(k):
        return [(2 * a + s, 2 * (a ^ k) + s) for a in range(levels) for s in range(2)]

    swap = [(i, i ^ 1) for i in range(members)]

    def across(k, s):
        return [
            (g * members + i, (g ^ k) * members + (i ^ s))
            for g in range(hosts)
            for i in range(members)
        ]

    ordered = []
    for chunk in chunks:
        starts = [(2 * a + side) * block for side in range(2) for a in chunk]
        ordered.append(jnp.concatenate([tokens[n : n + block] for n in starts], axis=0))
    level_parts = [
        [mine] + [lax.ppermute(mine, "tp", along(k)) for k in range(1, levels)]
        for mine in ordered
    ]
    gate_other = lax.ppermute(shared_gate, "tp", swap)
    up_other = lax.ppermute(shared_up, "tp", swap)
    route = []
    for chunk in chunks:
        route += [
            shape((hosts, rows), jnp.int32),
            shape((2 * hosts, rows // 2), jnp.int32),
            shape((2 * hosts, rows // 2), F32),
        ]
    params = [norm_gain.reshape(1, full), norm_shift.reshape(1, full), shared_gate, shared_up]
    route += [shape(p.shape, p.dtype) for p in params]
    route = call(
        functools.partial(route_body, block, cap, chunks),
        route,
        [expert_ids.T, affinity.T] + params,
    )
    gain, shift, gate_own, up_own = route[-4:]

    slots_of, hidden_of = [], []
    for q in range(len(chunks)):
        parts = []
        for n, part in enumerate(level_parts[q]):
            if n or q:
                after = hidden_of[q - 1] if q else route[0]
                part = lax.optimization_barrier((part, after))[0]
            parts += [part, lax.ppermute(part, "tp", swap)]
        out = call(
            functools.partial(norm_body, hosts),
            [shape((members, 2 * per * cap, width), BF16) for _ in range(hosts)]
            + [shape((rows // 2, 2 * units), BF16)],
            parts + [gain, shift, route[3 * q], gate_own, up_own, gate_other, up_other],
        )
        slots_of.append(
            [out[0]]
            + [lax.ppermute(out[k], ("ep", "tp"), across(k, 0)) for k in range(1, hosts)]
        )
        hidden_of.append(out[hosts])

    returned_of = []
    for q in range(len(chunks)):
        out = call(
            functools.partial(expert_body, hosts),
            [shape((per * cap, full), BF16) for _ in range(2 * hosts)],
            slots_of[q] + [expert_gate, expert_up, expert_down],
            24,
            [
                pltpu.VMEM((hosts * 2 * per * cap, full), BF16),
                pltpu.VMEM(expert_down.shape[1:], BF16),
                pltpu.SemaphoreType.DMA(()),
            ],
            [VM] * (hosts + 2) + [pl.BlockSpec(memory_space=pltpu.HBM)],
        )
        returned_of.append(
            [out[0]]
            + [
                lax.ppermute(out[s * hosts + k], ("ep", "tp"), across(k, s))
                for s in range(2)
                for k in range(hosts)
                if s or k
            ]
        )

    sums = []
    for q, chunk in enumerate(chunks):
        out = call(
            functools.partial(combine_body, chunk),
            [shape((block, full), F32)] + [shape((block, full), BF16) for _ in range(levels - 1)],
            returned_of[q] + [route[3 * q + 1], route[3 * q + 2], hidden_of[q], shared_down],
            16,
            [pltpu.VMEM((rows // 2, full), F32)],
        )
        sums.append(out[0])
        for k in range(1, levels):
            pairs = [(2 * (a ^ k) + s, 2 * a + s) for a in chunk for s in range(2)]
            sums.append(lax.ppermute(out[k], "tp", pairs))
    return call(
        functools.partial(final_body, chunks), shape((block, full), BF16), sums
    )


def solution(mesh):
    placed = (
        P("ep", "tp"),
        P(),
        P(),
        P("ep", None),
        P("ep", None),
        P(("ep", "tp"), None, None),
        P(("ep", "tp"), None, None),
        P(("ep", "tp"), None, None),
        P("tp", None),
        P("tp", None),
        P(),
    )
    return jax.shard_map(
        on_device, mesh=mesh, in_specs=placed, out_specs=P(("ep", "tp"), None), check_vma=False
    )
```

time: 273 us -> 130 us (0.48)
  local copies, waits for them, and re-layouts: 71.2 us -> 7.22 us
  waiting for transfers between devices: 120 us -> 60 us
  starting transfers between devices: 9.63 us -> 47.9 us
  other arithmetic: 25.8 us -> 0.02 us
  matrix products: 19.9 us -> 0 us
  between operations: 13.8 us -> 0.21 us
  Pallas kernels: 0 us -> 12.3 us
  blocking collectives: 11.3 us -> 0 us
    all_to_all x2 -> x0, waiting for transfers between devices: 70.9 us -> none  [the longest x1 35.7 us: on_device(): lax.all_to_all(result.reshape(incoming.shape), 'ep', split_axis=0, concat...]
    ppermute x0 -> x42, waiting for transfers between devices: none -> 60 us  [the longest x6 25.5 us: on_device(): lax.ppermute(out[k], ('ep', 'tp'), across(k, 0))]
    gather x7 -> x0, local copies, waits for them, and re-layouts: 54.7 us -> none  [the longest x6 45.7 us: weighted_sum(): jnp.take(source_rows, slot_index[:, column], axis=0, mode='fill', fill_va...]
    ppermute x0 -> x42, starting transfers between devices: none -> 47.9 us  [the longest x14 14.7 us: on_device(): lax.ppermute(out[s * hosts + k], ('ep', 'tp'), across(k, s))]
    reduce_scatter x1 -> x0, waiting for transfers between devices: 34.9 us -> none  [on_device(): lax.psum_scatter(weighted_sum(back_rows, pair_slot, weights, top_count),...]
    dot_general x5 -> x0, matrix products: 19.9 us -> none  [the longest x1 8.18 us: expert_rows(): jnp.dot(hidden, w_down, preferred_element_type=jnp.float32)]
    all_gather x1 -> x0, waiting for transfers between devices: 13.8 us -> none  [on_device(): whole = lax.all_gather(tokens, 'tp', axis=1, tiled=True)]
    pallas_call x0 -> x8, Pallas kernels: none -> 12.3 us  [call(): pl.pallas_call(body, out_shape=outs, in_specs=specs or [VM] * len(operand...]
  transfers between devices with their start and end apart: 4 -> 42, of which waited for: 4 -> 18; matrix products, arithmetic and copies ran while one was open for 10% -> 0% of each run, Pallas kernels for 0% -> 7%
where the time goes in v1:
time: 130 us; the launch traced here: 128 us
  waiting for transfers between devices  60 us (46%)
  starting transfers between devices  47.9 us (37%)
  Pallas kernels  12.3 us (9%)
  local copies, waits for them, and re-layouts  7.22 us (6%)
    ppermute x6, waiting for transfers between devices, on_device(): lax.ppermute(out[k], ('ep', 'tp'), across(k, 0))  25.5 us
    ppermute x6, waiting for transfers between devices, on_device(): lax.ppermute(mine, 'tp', along(k))  14.9 us
    ppermute x14, starting transfers between devices, on_device(): lax.ppermute(out[s * hosts + k], ('ep', 'tp'), across(k, s))  14.7 us
    ppermute x6, starting transfers between devices, on_device(): sums.append(lax.ppermute(out[k], 'tp', pairs))  14.3 us
    pallas_call x8, Pallas kernels, call(): pl.pallas_call(body, out_shape=outs, in_specs=specs or [VM] * len(operand...  12.3 us
    ppermute x6, starting transfers between devices, on_device(): lax.ppermute(mine, 'tp', along(k))  10.2 us
    ppermute x14, waiting for transfers between devices, on_device(): lax.ppermute(out[s * hosts + k], ('ep', 'tp'), across(k, s))  9.79 us
    ppermute x6, waiting for transfers between devices, on_device(): sums.append(lax.ppermute(out[k], 'tp', pairs))  8.53 us
  transfers between devices with their start and end apart: 42, of which 18 were waited for; matrix products, arithmetic and copies ran while one was open for 0% of the time, Pallas kernels for 7%

profile of v1, /device:TPU:0, one launch (start us, length us, event | category | flops | bytes accessed | tf_op | source)
XLA Modules:
  0.0 127.7 jit_solution(16252452723730540990)
XLA Ops:
  0.0 0.9 fusion
  0.9 3.1 %collective-permute-start.1 = (bf16[256,256]{1,0:T(8,128)(2,1)S(1)}, bf16[256,256]{1,0:T(8,128)(2,1)S(1)}, u32[]{:S(2)}, u32[]{:S(2)}) collective-permute-start(bf16[256,256]{1,0:T(8,128)(2,1)S(1)} %pad_maximum_fusion.refs_0_), channel_id=1, source_target_pairs={{0,2},{1,3},{2,0},{3,1},{4,6},{5,7},{6,4},{7,5},{8,10},{9,11},{10,... | collective-permute-start | bytes 393224 | tf_op jit(solution)/shard_map/ppermute | solution.py:243
  4.0 2.6 %collective-permute-start.3 = (bf16[256,256]{1,0:T(8,128)(2,1)S(1)}, bf16[256,256]{1,0:T(8,128)(2,1)S(1)}, u32[]{:S(2)}, u32[]{:S(2)}) collective-permute-start(bf16[256,256]{1,0:T(8,128)(2,1)S(1)} %pad_maximum_fusion.refs_0_), channel_id=1, source_target_pairs={{0,4},{1,5},{2,6},{3,7},{4,0},{5,1},{6,2},{7,3},{8,12},{9,13},{10,... | collective-permute-start | bytes 393224 | tf_op jit(solution)/shard_map/ppermute | solution.py:243
  7.1 2.0 %collective-permute-done.1.refs_2_ = bf16[256,256]{1,0:T(8,128)(2,1)S(1)} collective-permute-done((bf16[256,256]{1,0:T(8,128)(2,1)S(1)}, bf16[256,256]{1,0:T(8,128)(2,1)S(1)}, u32[]{:S(2)}, u32[]{:S(2)}) %collective-permute-start.1) | collective-permute-done | bytes 131104 | tf_op jit(solution)/shard_map/ppermute | solution.py:243
  9.1 0.9 copy-done.5
  10.1 0.9 copy-done.6
  11.0 0.7 copy-done.7
  11.7 0.7 copy-done.8
  12.5 0.7 copy-done.9
  14.2 2.8 %collective-permute-done.3.refs_4_ = bf16[256,256]{1,0:T(8,128)(2,1)S(1)} collective-permute-done((bf16[256,256]{1,0:T(8,128)(2,1)S(1)}, bf16[256,256]{1,0:T(8,128)(2,1)S(1)}, u32[]{:S(2)}, u32[]{:S(2)}) %collective-permute-start.3) | collective-permute-done | bytes 131104 | tf_op jit(solution)/shard_map/ppermute | solution.py:243
  17.5 0.8 collective-permute-done.2.refs_3_
  18.8 2.0 %shard_map.110 = (bf16[8,96,256]{2,1,0:T(8,128)(2,1)S(1)}, bf16[8,96,256]{2,1,0:T(8,128)(2,1)S(1)}, bf16[8,96,256]{2,1,0:T(8,128)(2,1)S(1)}, bf16[8,96,256]{2,1,0:T(8,128)(2,1)S(1)}, bf16[128,128]{1,0:T(8,128)(2,1)S(1)}) custom-call(bf16[256,256]{1,0:T(8,128)(2,1)S(1)} %pad_maximum_fusion.refs_0_, bf16[256,256]{1,0:T(8,128)(2,1)S(1)} %collective-permute-done.refs_1_, ...), custom_call_target="tpu_custom_call" | custom-call | tf_op jit(solution)/shard_map/pallas_call | solution.py:22
  20.8 1.6 %collective-permute-start.9 = (bf16[8,96,256]{2,1,0:T(8,128)(2,1)S(1)}, bf16[8,96,256]{2,1,0:T(8,128)(2,1)S(1)}, u32[]{:S(2)}, u32[]{:S(2)}) collective-permute-start(bf16[8,96,256]{2,1,0:T(8,128)(2,1)S(1)} %get-tuple-element.65), channel_id=1, source_target_pairs={{0,8},{1,9},{2,10},{3,11},{4,12},{5,13},{6,14},{7,15},{8,0},{9,1},... | collective-permute-start | bytes 1179656 | tf_op jit(solution)/shard_map/ppermute | solution.py:280
  22.4 1.7 %collective-permute-start.23 = (bf16[256,256]{1,0:T(8,128)(2,1)S(1)}, bf16[256,256]{1,0:T(8,128)(2,1)S(1)}, u32[]{:S(2)}, u32[]{:S(2)}) collective-permute-start(bf16[256,256]{1,0:T(8,128)(2,1)S(1)} %pad_maximum_fusion.1.refs_0_), channel_id=1, source_target_pairs={{0,2},{1,3},{2,0},{3,1},{4,6},{5,7},{6,4},{7,5},{8,10},{9,11},{10,... | collective-permute-start | bytes 393224 | tf_op jit(solution)/shard_map/ppermute | solution.py:243
  24.1 1.2 collective-permute-start.25
  25.3 1.5 %collective-permute-start.27 = (bf16[256,256]{1,0:T(8,128)(2,1)S(1)}, bf16[256,256]{1,0:T(8,128)(2,1)S(1)}, u32[]{:S(2)}, u32[]{:S(2)}) collective-permute-start(bf16[256,256]{1,0:T(8,128)(2,1)S(1)} %pad_maximum_fusion.1.refs_0_), channel_id=1, source_target_pairs={{0,6},{1,7},{2,4},{3,5},{4,2},{5,3},{6,0},{7,1},{8,14},{9,15},{10,... | collective-permute-start | bytes 393224 | tf_op jit(solution)/shard_map/ppermute | solution.py:243
  26.8 2.8 %collective-permute-done.23.refs_2_ = bf16[256,256]{1,0:T(8,128)(2,1)S(1)} collective-permute-done((bf16[256,256]{1,0:T(8,128)(2,1)S(1)}, bf16[256,256]{1,0:T(8,128)(2,1)S(1)}, u32[]{:S(2)}, u32[]{:S(2)}) %collective-permute-start.23) | collective-permute-done | bytes 131104 | tf_op jit(solution)/shard_map/ppermute | solution.py:243
  29.6 7.4 %collective-permute-done.25.refs_4_ = bf16[256,256]{1,0:T(8,128)(2,1)S(1)} collective-permute-done((bf16[256,256]{1,0:T(8,128)(2,1)S(1)}, bf16[256,256]{1,0:T(8,128)(2,1)S(1)}, u32[]{:S(2)}, u32[]{:S(2)}) %collective-permute-start.25) | collective-permute-done | bytes 131104 | tf_op jit(solution)/shard_map/ppermute | solution.py:243
  37.5 1.5 %collective-permute-start.10 = (bf16[8,96,256]{2,1,0:T(8,128)(2,1)S(1)}, bf16[8,96,256]{2,1,0:T(8,128)(2,1)S(1)}, u32[]{:S(2)}, u32[]{:S(2)}) collective-permute-start(bf16[8,96,256]{2,1,0:T(8,128)(2,1)S(1)} %get-tuple-element.66), channel_id=1, source_target_pairs={{0,16},{1,17},{2,18},{3,19},{4,20},{5,21},{6,22},{7,23},{8,24},{9,... | collective-permute-start | bytes 1179656 | tf_op jit(solution)/shard_map/ppermute | solution.py:280
  39.5 2.0 %shard_map.113 = (bf16[8,96,256]{2,1,0:T(8,128)(2,1)S(1)}, bf16[8,96,256]{2,1,0:T(8,128)(2,1)S(1)}, bf16[8,96,256]{2,1,0:T(8,128)(2,1)S(1)}, bf16[8,96,256]{2,1,0:T(8,128)(2,1)S(1)}, bf16[128,128]{1,0:T(8,128)(2,1)S(1)}) custom-call(bf16[256,256]{1,0:T(8,128)(2,1)S(1)} %pad_maximum_fusion.1.refs_0_, bf16[256,256]{1,0:T(8,128)(2,1)S(1)} %collective-permute-done.22.refs_1_, ...), custom_call_target="tpu_custom_call" | custom-call | tf_op jit(solution)/shard_map/pallas_call | solution.py:22
  41.5 1.6 %collective-permute-start.29 = (bf16[8,96,256]{2,1,0:T(8,128)(2,1)S(1)}, bf16[8,96,256]{2,1,0:T(8,128)(2,1)S(1)}, u32[]{:S(2)}, u32[]{:S(2)}) collective-permute-start(bf16[8,96,256]{2,1,0:T(8,128)(2,1)S(1)} %get-tuple-element.89), channel_id=1, source_target_pairs={{0,8},{1,9},{2,10},{3,11},{4,12},{5,13},{6,14},{7,15},{8,0},{9,1},... | collective-permute-start | bytes 1179656 | tf_op jit(solution)/shard_map/ppermute | solution.py:280
  43.1 1.5 %collective-permute-start.30 = (bf16[8,96,256]{2,1,0:T(8,128)(2,1)S(1)}, bf16[8,96,256]{2,1,0:T(8,128)(2,1)S(1)}, u32[]{:S(2)}, u32[]{:S(2)}) collective-permute-start(bf16[8,96,256]{2,1,0:T(8,128)(2,1)S(1)} %get-tuple-element.90), channel_id=1, source_target_pairs={{0,16},{1,17},{2,18},{3,19},{4,20},{5,21},{6,22},{7,23},{8,24},{9,... | collective-permute-start | bytes 1179656 | tf_op jit(solution)/shard_map/ppermute | solution.py:280
  45.1 12.9 %collective-permute-done.10.refs_2_ = bf16[8,96,256]{2,1,0:T(8,128)(2,1)S(1)} collective-permute-done((bf16[8,96,256]{2,1,0:T(8,128)(2,1)S(1)}, bf16[8,96,256]{2,1,0:T(8,128)(2,1)S(1)}, u32[]{:S(2)}, u32[]{:S(2)}) %collective-permute-start.10) | collective-permute-done | bytes 393248 | tf_op jit(solution)/shard_map/ppermute | solution.py:280
  58.0 1.6 %copy-done.3 = bf16[1,512,2048]{2,1,0:T(8,128)(2,1)S(1)} copy-done((bf16[1,512,2048]{2,1,0:T(8,128)(2,1)S(1)}, bf16[1,512,2048]{2,1,0:T(8,128)(2,1)}, u32[]{:S(2)}) %copy-start.3) | copy-done | bytes 2097176
  59.5 2.9 %shard_map.111 = (bf16[48,2048]{1,0:T(8,128)(2,1)S(1)}, bf16[48,2048]{1,0:T(8,128)(2,1)S(1)}, bf16[48,2048]{1,0:T(8,128)(2,1)S(1)}, bf16[48,2048]{1,0:T(8,128)(2...) custom-call(bf16[8,96,256]{2,1,0:T(8,128)(2,1)S(1)} %get-tuple-eleme, ...), custom_call_target="tpu_custom_call" | custom-call | tf_op jit(solution)/shard_map/pallas_call | solution.py:22
  63.1 2.4 %collective-permute-start.13 = (bf16[48,2048]{1,0:T(8,128)(2,1)S(1)}, bf16[48,2048]{1,0:T(8,128)(2,1)S(1)}, u32[]{:S(2)}, u32[]{:S(2)}) collective-permute-start(bf16[48,2048]{1,0:T(8,128)(2,1)S(1)} %get-tuple-element.70), channel_id=1, source_target_pairs={{0,16},{1,17},{2,18},{3,19},{4,20},{5,21},{6,22},{7,23},{8,24},{9,... | collective-permute-start | bytes 589832 | tf_op jit(solution)/shard_map/ppermute | solution.py:301
  65.4 0.9 collective-permute-start.14
  66.4 12.6 %collective-permute-done.30.refs_2_ = bf16[8,96,256]{2,1,0:T(8,128)(2,1)S(1)} collective-permute-done((bf16[8,96,256]{2,1,0:T(8,128)(2,1)S(1)}, bf16[8,96,256]{2,1,0:T(8,128)(2,1)S(1)}, u32[]{:S(2)}, u32[]{:S(2)}) %collective-permute-start.30) | collective-permute-done | bytes 393248 | tf_op jit(solution)/shard_map/ppermute | solution.py:280
  79.7 1.1 collective-permute-start.17
  80.8 1.5 %collective-permute-done.13.refs_2_ = bf16[48,2048]{1,0:T(8,128)(2,1)S(1)} collective-permute-done((bf16[48,2048]{1,0:T(8,128)(2,1)S(1)}, bf16[48,2048]{1,0:T(8,128)(2,1)S(1)}, u32[]{:S(2)}, u32[]{:S(2)}) %collective-permute-start.13) | collective-permute-done | bytes 196640 | tf_op jit(solution)/shard_map/ppermute | solution.py:301
  82.6 2.9 %shard_map.114 = (bf16[48,2048]{1,0:T(8,128)(2,1)S(1)}, bf16[48,2048]{1,0:T(8,128)(2,1)S(1)}, bf16[48,2048]{1,0:T(8,128)(2,1)S(1)}, bf16[48,2048]{1,0:T(8,128)(2...) custom-call(bf16[8,96,256]{2,1,0:T(8,128)(2,1)S(1)} %get-tuple-eleme, ...), custom_call_target="tpu_custom_call" | custom-call | tf_op jit(solution)/shard_map/pallas_call | solution.py:22
  85.6 1.6 %collective-permute-start.32 = (bf16[48,2048]{1,0:T(8,128)(2,1)S(1)}, bf16[48,2048]{1,0:T(8,128)(2,1)S(1)}, u32[]{:S(2)}, u32[]{:S(2)}) collective-permute-start(bf16[48,2048]{1,0:T(8,128)(2,1)S(1)} %get-tuple-element.93), channel_id=1, source_target_pairs={{0,8},{1,9},{2,10},{3,11},{4,12},{5,13},{6,14},{7,15},{8,0},{9,1},... | collective-permute-start | bytes 589832 | tf_op jit(solution)/shard_map/ppermute | solution.py:301
  87.6 1.5 %collective-permute-start.34 = (bf16[48,2048]{1,0:T(8,128)(2,1)S(1)}, bf16[48,2048]{1,0:T(8,128)(2,1)S(1)}, u32[]{:S(2)}, u32[]{:S(2)}) collective-permute-start(bf16[48,2048]{1,0:T(8,128)(2,1)S(1)} %get-tuple-element.95), channel_id=1, source_target_pairs={{0,24},{1,25},{2,26},{3,27},{4,28},{5,29},{6,30},{7,31},{8,16},{9,... | collective-permute-start | bytes 589832 | tf_op jit(solution)/shard_map/ppermute | solution.py:301
  89.1 1.0 collective-permute-done.17.refs_6_
  91.4 1.3 %collective-permute-start.19 = (bf16[64,2048]{1,0:T(8,128)(2,1)S(1)}, bf16[64,2048]{1,0:T(8,128)(2,1)S(1)}, u32[]{:S(2)}, u32[]{:S(2)}) collective-permute-start(bf16[64,2048]{1,0:T(8,128)(2,1)S(1)} %get-tuple-element.80), channel_id=1, source_target_pairs={{2,0},{3,1},{4,6},{5,7},{10,8},{11,9},{12,14},{13,15},{18,16},{19,... | collective-permute-start | bytes 786440 | tf_op jit(solution)/shard_map/ppermute | solution.py:320
  92.7 1.3 collective-permute-start.35
  95.0 3.6 %collective-permute-done.33.refs_2_ = bf16[48,2048]{1,0:T(8,128)(2,1)S(1)} collective-permute-done((bf16[48,2048]{1,0:T(8,128)(2,1)S(1)}, bf16[48,2048]{1,0:T(8,128)(2,1)S(1)}, u32[]{:S(2)}, u32[]{:S(2)}) %collective-permute-start.33) | collective-permute-done | bytes 196640 | tf_op jit(solution)/shard_map/ppermute | solution.py:301
  98.6 2.0 %collective-permute-start.37 = (bf16[48,2048]{1,0:T(8,128)(2,1)S(1)}, bf16[48,2048]{1,0:T(8,128)(2,1)S(1)}, u32[]{:S(2)}, u32[]{:S(2)}) collective-permute-start(bf16[48,2048]{1,0:T(8,128)(2,1)S(1)} %get-tuple-element.98), channel_id=1, source_target_pairs={{0,17},{1,16},{2,19},{3,18},{4,21},{5,20},{6,23},{7,22},{8,25},{9,... | collective-permute-start | bytes 589832 | tf_op jit(solution)/shard_map/ppermute | solution.py:301
  100.6 1.6 %collective-permute-start.38 = (bf16[48,2048]{1,0:T(8,128)(2,1)S(1)}, bf16[48,2048]{1,0:T(8,128)(2,1)S(1)}, u32[]{:S(2)}, u32[]{:S(2)}) collective-permute-start(bf16[48,2048]{1,0:T(8,128)(2,1)S(1)} %get-tuple-element.99), channel_id=1, source_target_pairs={{0,25},{1,24},{2,27},{3,26},{4,29},{5,28},{6,31},{7,30},{8,17},{9,... | collective-permute-start | bytes 589832 | tf_op jit(solution)/shard_map/ppermute | solution.py:301
  102.1 1.3 %collective-permute-start.20 = (bf16[64,2048]{1,0:T(8,128)(2,1)S(1)}, bf16[64,2048]{1,0:T(8,128)(2,1)S(1)}, u32[]{:S(2)}, u32[]{:S(2)}) collective-permute-start(bf16[64,2048]{1,0:T(8,128)(2,1)S(1)} %get-tuple-element.81), channel_id=1, source_target_pairs={{4,0},{5,1},{2,6},{3,7},{12,8},{13,9},{10,14},{11,15},{20,16},{21,... | collective-permute-start | bytes 786440 | tf_op jit(solution)/shard_map/ppermute | solution.py:320
  103.4 4.1 %collective-permute-start.21 = (bf16[64,2048]{1,0:T(8,128)(2,1)S(1)}, bf16[64,2048]{1,0:T(8,128)(2,1)S(1)}, u32[]{:S(2)}, u32[]{:S(2)}) collective-permute-start(bf16[64,2048]{1,0:T(8,128)(2,1)S(1)} %get-tuple-element.82), channel_id=1, source_target_pairs={{6,0},{7,1},{0,6},{1,7},{14,8},{15,9},{8,14},{9,15},{22,16},{23,17... | collective-permute-start | bytes 786440 | tf_op jit(solution)/shard_map/ppermute | solution.py:320
  107.5 2.4 %collective-permute-done.37.refs_6_ = bf16[48,2048]{1,0:T(8,128)(2,1)S(1)} collective-permute-done((bf16[48,2048]{1,0:T(8,128)(2,1)S(1)}, bf16[48,2048]{1,0:T(8,128)(2,1)S(1)}, u32[]{:S(2)}, u32[]{:S(2)}) %collective-permute-start.37) | collective-permute-done | bytes 196640 | tf_op jit(solution)/shard_map/ppermute | solution.py:301
  110.0 0.7 shard_map.115
  110.7 4.7 %collective-permute-start.39 = (bf16[64,2048]{1,0:T(8,128)(2,1)S(1)}, bf16[64,2048]{1,0:T(8,128)(2,1)S(1)}, u32[]{:S(2)}, u32[]{:S(2)}) collective-permute-start(bf16[64,2048]{1,0:T(8,128)(2,1)S(1)} %get-tuple-element.104), channel_id=1, source_target_pairs={{0,2},{1,3},{6,4},{7,5},{8,10},{9,11},{14,12},{15,13},{16,18},{17,... | collective-permute-start | bytes 786440 | tf_op jit(solution)/shard_map/ppermute | solution.py:320
  115.4 2.3 %collective-permute-start.40 = (bf16[64,2048]{1,0:T(8,128)(2,1)S(1)}, bf16[64,2048]{1,0:T(8,128)(2,1)S(1)}, u32[]{:S(2)}, u32[]{:S(2)}) collective-permute-start(bf16[64,2048]{1,0:T(8,128)(2,1)S(1)} %get-tuple-element.105), channel_id=1, source_target_pairs={{6,2},{7,3},{0,4},{1,5},{14,10},{15,11},{8,12},{9,13},{22,18},{23,... | collective-permute-start | bytes 786440 | tf_op jit(solution)/shard_map/ppermute | solution.py:320
  118.7 3.4 %collective-permute-done.39.refs_5_ = bf16[64,2048]{1,0:T(8,128)(2,1)S(1)} collective-permute-done((bf16[64,2048]{1,0:T(8,128)(2,1)S(1)}, bf16[64,2048]{1,0:T(8,128)(2,1)S(1)}, u32[]{:S(2)}, u32[]{:S(2)}) %collective-permute-start.39) | collective-permute-done | bytes 262176 | tf_op jit(solution)/shard_map/ppermute | solution.py:320
  122.1 4.8 %collective-permute-done.40.refs_6_ = bf16[64,2048]{1,0:T(8,128)(2,1)S(1)} collective-permute-done((bf16[64,2048]{1,0:T(8,128)(2,1)S(1)}, bf16[64,2048]{1,0:T(8,128)(2,1)S(1)}, u32[]{:S(2)}, u32[]{:S(2)}) %collective-permute-start.40) | collective-permute-done | bytes 262176 | tf_op jit(solution)/shard_map/ppermute | solution.py:320
  126.9 0.8 shard_map.116
  (69 shorter events, 9.5 us)
Async XLA Ops:
  0.9 8.2 %collective-permute-start.1 = (bf16[256,256]{1,0:T(8,128)(2,1)S(1)}, bf16[256,256]{1,0:T(8,128)(2,1)S(1)}, u32[]{:S(2)}, u32[]{:S(2)}) collective-permute-start(bf16[256,256]{1,0:T(8,128)(2,1)S(1)} %pad_maximum_fusion.refs_0_), channel_id=1, source_target_pairs={{0,2},{1,3},{2,0},{3,1},{4,6},{5,7},{6,4},{7,5},{8,10},{9,11},{10,... | collective-permute-start | bytes 393224 | tf_op jit(solution)/shard_map/ppermute | solution.py:243
  4.0 12.9 %collective-permute-start.3 = (bf16[256,256]{1,0:T(8,128)(2,1)S(1)}, bf16[256,256]{1,0:T(8,128)(2,1)S(1)}, u32[]{:S(2)}, u32[]{:S(2)}) collective-permute-start(bf16[256,256]{1,0:T(8,128)(2,1)S(1)} %pad_maximum_fusion.refs_0_), channel_id=1, source_target_pairs={{0,4},{1,5},{2,6},{3,7},{4,0},{5,1},{6,2},{7,3},{8,12},{9,13},{10,... | collective-permute-start | bytes 393224 | tf_op jit(solution)/shard_map/ppermute | solution.py:243
  6.6 10.3 %collective-permute-start.5 = (bf16[256,256]{1,0:T(8,128)(2,1)S(1)}, bf16[256,256]{1,0:T(8,128)(2,1)S(1)}, u32[]{:S(2)}, u32[]{:S(2)}) collective-permute-start(bf16[256,256]{1,0:T(8,128)(2,1)S(1)} %pad_maximum_fusion.refs_0_), channel_id=1, source_target_pairs={{0,6},{1,7},{2,4},{3,5},{4,2},{5,3},{6,0},{7,1},{8,14},{9,15},{10,... | collective-permute-start | bytes 393224 | tf_op jit(solution)/shard_map/ppermute | solution.py:243
  6.6 10.8 %collective-permute-start = (bf16[256,256]{1,0:T(8,128)(2,1)S(1)}, bf16[256,256]{1,0:T(8,128)(2,1)S(1)}, u32[]{:S(2)}, u32[]{:S(2)}) collective-permute-start(bf16[256,256]{1,0:T(8,128)(2,1)S(1)} %pad_maximum_fusion.refs_0_), channel_id=1, source_target_pairs={{0,1},{1,0},{2,3},{3,2},{4,5},{5,4},{6,7},{7,6},{8,9},{9,8},{10,11... | collective-permute-start | bytes 393224 | tf_op jit(solution)/shard_map/ppermute | solution.py:271
  6.6 12.2 %collective-permute-start.7 = (bf16[64,2048]{1,0:T(8,128)(2,1)}, bf16[64,2048]{1,0:T(8,128)(2,1)S(1)}, u32[]{:S(2)}, u32[]{:S(2)}) collective-permute-start(bf16[64,2048]{1,0:T(8,128)(2,1)} %rest_2_.1), channel_id=1, source_target_pairs={{0,1},{1,0},{2,3},{3,2},{4,5},{5,4},{6,7},{7,6},{8,9},{9,8},{10,11... | collective-permute-start | bytes 786440 | tf_op jit(solution)/shard_map/ppermute | solution.py:246
  9.1 9.7 %collective-permute-start.8 = (bf16[64,2048]{1,0:T(8,128)(2,1)}, bf16[64,2048]{1,0:T(8,128)(2,1)S(1)}, u32[]{:S(2)}, u32[]{:S(2)}) collective-permute-start(bf16[64,2048]{1,0:T(8,128)(2,1)} %rest_3_.1), channel_id=1, source_target_pairs={{0,1},{1,0},{2,3},{3,2},{4,5},{5,4},{6,7},{7,6},{8,9},{9,8},{10,11... | collective-permute-start | bytes 786440 | tf_op jit(solution)/shard_map/ppermute | solution.py:247
  9.1 1.0 copy-start.5
  16.9 1.3 %collective-permute-start.2 = (bf16[256,256]{1,0:T(8,128)(2,1)S(1)}, bf16[256,256]{1,0:T(8,128)(2,1)S(1)}, u32[]{:S(2)}, u32[]{:S(2)}) collective-permute-start(bf16[256,256]{1,0:T(8,128)(2,1)S(1)} %collective-permute-done.1.refs_2_), channel_id=1, source_target_pairs={{0,1},{1,0},{2,3},{3,2},{4,5},{5,4},{6,7},{7,6},{8,9},{9,8},{10,11... | collective-permute-start | bytes 393224 | tf_op jit(solution)/shard_map/ppermute | solution.py:271
  16.9 1.5 %collective-permute-start.4 = (bf16[256,256]{1,0:T(8,128)(2,1)S(1)}, bf16[256,256]{1,0:T(8,128)(2,1)S(1)}, u32[]{:S(2)}, u32[]{:S(2)}) collective-permute-start(bf16[256,256]{1,0:T(8,128)(2,1)S(1)} %collective-permute-done.3.refs_4_), channel_id=1, source_target_pairs={{0,1},{1,0},{2,3},{3,2},{4,5},{5,4},{6,7},{7,6},{8,9},{9,8},{10,11... | collective-permute-start | bytes 393224 | tf_op jit(solution)/shard_map/ppermute | solution.py:271
  17.4 1.3 %collective-permute-start.6 = (bf16[256,256]{1,0:T(8,128)(2,1)S(1)}, bf16[256,256]{1,0:T(8,128)(2,1)S(1)}, u32[]{:S(2)}, u32[]{:S(2)}) collective-permute-start(bf16[256,256]{1,0:T(8,128)(2,1)S(1)} %collective-permute-done.5.refs_6_), channel_id=1, source_target_pairs={{0,1},{1,0},{2,3},{3,2},{4,5},{5,4},{6,7},{7,6},{8,9},{9,8},{10,11... | collective-permute-start | bytes 393224 | tf_op jit(solution)/shard_map/ppermute | solution.py:271
  18.8 39.1 %copy-start.1 = (bf16[1,2048,512]{2,1,0:T(8,128)(2,1)S(1)}, bf16[1,2048,512]{2,1,0:T(8,128)(2,1)}, u32[]{:S(2)}) copy-start(bf16[1,2048,512]{2,1,0:T(8,128)(2,1)} %refs_4_.3) | copy-start | bytes 6291460
  18.8 39.1 %copy-start.2 = (bf16[1,2048,512]{2,1,0:T(8,128)(2,1)S(1)}, bf16[1,2048,512]{2,1,0:T(8,128)(2,1)}, u32[]{:S(2)}) copy-start(bf16[1,2048,512]{2,1,0:T(8,128)(2,1)} %refs_5_.3) | copy-start | bytes 6291460
  20.8 23.8 %collective-permute-start.9 = (bf16[8,96,256]{2,1,0:T(8,128)(2,1)S(1)}, bf16[8,96,256]{2,1,0:T(8,128)(2,1)S(1)}, u32[]{:S(2)}, u32[]{:S(2)}) collective-permute-start(bf16[8,96,256]{2,1,0:T(8,128)(2,1)S(1)} %get-tuple-element.65), channel_id=1, source_target_pairs={{0,8},{1,9},{2,10},{3,11},{4,12},{5,13},{6,14},{7,15},{8,0},{9,1},... | collective-permute-start | bytes 1179656 | tf_op jit(solution)/shard_map/ppermute | solution.py:280
  22.4 7.2 %collective-permute-start.23 = (bf16[256,256]{1,0:T(8,128)(2,1)S(1)}, bf16[256,256]{1,0:T(8,128)(2,1)S(1)}, u32[]{:S(2)}, u32[]{:S(2)}) collective-permute-start(bf16[256,256]{1,0:T(8,128)(2,1)S(1)} %pad_maximum_fusion.1.refs_0_), channel_id=1, source_target_pairs={{0,2},{1,3},{2,0},{3,1},{4,6},{5,7},{6,4},{7,5},{8,10},{9,11},{10,... | collective-permute-start | bytes 393224 | tf_op jit(solution)/shard_map/ppermute | solution.py:243
  24.1 12.9 %collective-permute-start.25 = (bf16[256,256]{1,0:T(8,128)(2,1)S(1)}, bf16[256,256]{1,0:T(8,128)(2,1)S(1)}, u32[]{:S(2)}, u32[]{:S(2)}) collective-permute-start(bf16[256,256]{1,0:T(8,128)(2,1)S(1)} %pad_maximum_fusion.1.refs_0_), channel_id=1, source_target_pairs={{0,4},{1,5},{2,6},{3,7},{4,0},{5,1},{6,2},{7,3},{8,12},{9,13},{10,... | collective-permute-start | bytes 393224 | tf_op jit(solution)/shard_map/ppermute | solution.py:243
  25.3 11.7 %collective-permute-start.27 = (bf16[256,256]{1,0:T(8,128)(2,1)S(1)}, bf16[256,256]{1,0:T(8,128)(2,1)S(1)}, u32[]{:S(2)}, u32[]{:S(2)}) collective-permute-start(bf16[256,256]{1,0:T(8,128)(2,1)S(1)} %pad_maximum_fusion.1.refs_0_), channel_id=1, source_target_pairs={{0,6},{1,7},{2,4},{3,5},{4,2},{5,3},{6,0},{7,1},{8,14},{9,15},{10,... | collective-permute-start | bytes 393224 | tf_op jit(solution)/shard_map/ppermute | solution.py:243
  26.8 10.7 %collective-permute-start.22 = (bf16[256,256]{1,0:T(8,128)(2,1)S(1)}, bf16[256,256]{1,0:T(8,128)(2,1)S(1)}, u32[]{:S(2)}, u32[]{:S(2)}) collective-permute-start(bf16[256,256]{1,0:T(8,128)(2,1)S(1)} %pad_maximum_fusion.1.refs_0_), channel_id=1, source_target_pairs={{0,1},{1,0},{2,3},{3,2},{4,5},{5,4},{6,7},{7,6},{8,9},{9,8},{10,11... | collective-permute-start | bytes 393224 | tf_op jit(solution)/shard_map/ppermute | solution.py:271
  29.6 9.4 %collective-permute-start.24 = (bf16[256,256]{1,0:T(8,128)(2,1)S(1)}, bf16[256,256]{1,0:T(8,128)(2,1)S(1)}, u32[]{:S(2)}, u32[]{:S(2)}) collective-permute-start(bf16[256,256]{1,0:T(8,128)(2,1)S(1)} %collective-permute-done.23.refs_2_), channel_id=1, source_target_pairs={{0,1},{1,0},{2,3},{3,2},{4,5},{5,4},{6,7},{7,6},{8,9},{9,8},{10,11... | collective-permute-start | bytes 393224 | tf_op jit(solution)/shard_map/ppermute | solution.py:271
  37.0 2.5 %collective-permute-start.26 = (bf16[256,256]{1,0:T(8,128)(2,1)S(1)}, bf16[256,256]{1,0:T(8,128)(2,1)S(1)}, u32[]{:S(2)}, u32[]{:S(2)}) collective-permute-start(bf16[256,256]{1,0:T(8,128)(2,1)S(1)} %collective-permute-done.25.refs_4_), channel_id=1, source_target_pairs={{0,1},{1,0},{2,3},{3,2},{4,5},{5,4},{6,7},{7,6},{8,9},{9,8},{10,11... | collective-permute-start | bytes 393224 | tf_op jit(solution)/shard_map/ppermute | solution.py:271
  37.0 2.5 %collective-permute-start.28 = (bf16[256,256]{1,0:T(8,128)(2,1)S(1)}, bf16[256,256]{1,0:T(8,128)(2,1)S(1)}, u32[]{:S(2)}, u32[]{:S(2)}) collective-permute-start(bf16[256,256]{1,0:T(8,128)(2,1)S(1)} %collective-permute-done.27.refs_6_), channel_id=1, source_target_pairs={{0,1},{1,0},{2,3},{3,2},{4,5},{5,4},{6,7},{7,6},{8,9},{9,8},{10,11... | collective-permute-start | bytes 393224 | tf_op jit(solution)/shard_map/ppermute | solution.py:271
  37.5 20.4 %collective-permute-start.10 = (bf16[8,96,256]{2,1,0:T(8,128)(2,1)S(1)}, bf16[8,96,256]{2,1,0:T(8,128)(2,1)S(1)}, u32[]{:S(2)}, u32[]{:S(2)}) collective-permute-start(bf16[8,96,256]{2,1,0:T(8,128)(2,1)S(1)} %get-tuple-element.66), channel_id=1, source_target_pairs={{0,16},{1,17},{2,18},{3,19},{4,20},{5,21},{6,22},{7,23},{8,24},{9,... | collective-permute-start | bytes 1179656 | tf_op jit(solution)/shard_map/ppermute | solution.py:280
  39.0 18.9 %collective-permute-start.11 = (bf16[8,96,256]{2,1,0:T(8,128)(2,1)S(1)}, bf16[8,96,256]{2,1,0:T(8,128)(2,1)S(1)}, u32[]{:S(2)}, u32[]{:S(2)}) collective-permute-start(bf16[8,96,256]{2,1,0:T(8,128)(2,1)S(1)} %get-tuple-element.67), channel_id=1, source_target_pairs={{0,24},{1,25},{2,26},{3,27},{4,28},{5,29},{6,30},{7,31},{8,16},{9,... | collective-permute-start | bytes 1179656 | tf_op jit(solution)/shard_map/ppermute | solution.py:280
  41.5 23.9 %collective-permute-start.29 = (bf16[8,96,256]{2,1,0:T(8,128)(2,1)S(1)}, bf16[8,96,256]{2,1,0:T(8,128)(2,1)S(1)}, u32[]{:S(2)}, u32[]{:S(2)}) collective-permute-start(bf16[8,96,256]{2,1,0:T(8,128)(2,1)S(1)} %get-tuple-element.89), channel_id=1, source_target_pairs={{0,8},{1,9},{2,10},{3,11},{4,12},{5,13},{6,14},{7,15},{8,0},{9,1},... | collective-permute-start | bytes 1179656 | tf_op jit(solution)/shard_map/ppermute | solution.py:280
  43.1 35.9 %collective-permute-start.30 = (bf16[8,96,256]{2,1,0:T(8,128)(2,1)S(1)}, bf16[8,96,256]{2,1,0:T(8,128)(2,1)S(1)}, u32[]{:S(2)}, u32[]{:S(2)}) collective-permute-start(bf16[8,96,256]{2,1,0:T(8,128)(2,1)S(1)} %get-tuple-element.90), channel_id=1, source_target_pairs={{0,16},{1,17},{2,18},{3,19},{4,20},{5,21},{6,22},{7,23},{8,24},{9,... | collective-permute-start | bytes 1179656 | tf_op jit(solution)/shard_map/ppermute | solution.py:280
  44.6 34.4 %collective-permute-start.31 = (bf16[8,96,256]{2,1,0:T(8,128)(2,1)S(1)}, bf16[8,96,256]{2,1,0:T(8,128)(2,1)S(1)}, u32[]{:S(2)}, u32[]{:S(2)}) collective-permute-start(bf16[8,96,256]{2,1,0:T(8,128)(2,1)S(1)} %get-tuple-element.91), channel_id=1, source_target_pairs={{0,24},{1,25},{2,26},{3,27},{4,28},{5,29},{6,30},{7,31},{8,16},{9,... | collective-permute-start | bytes 1179656 | tf_op jit(solution)/shard_map/ppermute | solution.py:280
  57.9 1.6 %copy-start.3 = (bf16[1,512,2048]{2,1,0:T(8,128)(2,1)S(1)}, bf16[1,512,2048]{2,1,0:T(8,128)(2,1)}, u32[]{:S(2)}) copy-start(bf16[1,512,2048]{2,1,0:T(8,128)(2,1)} %refs_6_.3) | copy-start | bytes 6291460
  59.5 23.1 %copy-start.4 = (bf16[1,512,2048]{2,1,0:T(8,128)(2,1)S(1)}, bf16[1,512,2048]{2,1,0:T(8,128)(2,1)}, u32[]{:S(2)}) copy-start(bf16[1,512,2048]{2,1,0:T(8,128)(2,1)} %refs_6_.3) | copy-start | bytes 6291460
  62.5 17.2 %collective-permute-start.12 = (bf16[48,2048]{1,0:T(8,128)(2,1)S(1)}, bf16[48,2048]{1,0:T(8,128)(2,1)S(1)}, u32[]{:S(2)}, u32[]{:S(2)}) collective-permute-start(bf16[48,2048]{1,0:T(8,128)(2,1)S(1)} %get-tuple-element.69), channel_id=1, source_target_pairs={{0,8},{1,9},{2,10},{3,11},{4,12},{5,13},{6,14},{7,15},{8,0},{9,1},... | collective-permute-start | bytes 589832 | tf_op jit(solution)/shard_map/ppermute | solution.py:301
  63.1 19.2 %collective-permute-start.13 = (bf16[48,2048]{1,0:T(8,128)(2,1)S(1)}, bf16[48,2048]{1,0:T(8,128)(2,1)S(1)}, u32[]{:S(2)}, u32[]{:S(2)}) collective-permute-start(bf16[48,2048]{1,0:T(8,128)(2,1)S(1)} %get-tuple-element.70), channel_id=1, source_target_pairs={{0,16},{1,17},{2,18},{3,19},{4,20},{5,21},{6,22},{7,23},{8,24},{9,... | collective-permute-start | bytes 589832 | tf_op jit(solution)/shard_map/ppermute | solution.py:301
  65.4 20.1 %collective-permute-start.14 = (bf16[48,2048]{1,0:T(8,128)(2,1)S(1)}, bf16[48,2048]{1,0:T(8,128)(2,1)S(1)}, u32[]{:S(2)}, u32[]{:S(2)}) collective-permute-start(bf16[48,2048]{1,0:T(8,128)(2,1)S(1)} %get-tuple-element.71), channel_id=1, source_target_pairs={{0,24},{1,25},{2,26},{3,27},{4,28},{5,29},{6,30},{7,31},{8,16},{9,... | collective-permute-start | bytes 589832 | tf_op jit(solution)/shard_map/ppermute | solution.py:301
  79.0 8.1 %collective-permute-start.15 = (bf16[48,2048]{1,0:T(8,128)(2,1)S(1)}, bf16[48,2048]{1,0:T(8,128)(2,1)S(1)}, u32[]{:S(2)}, u32[]{:S(2)}) collective-permute-start(bf16[48,2048]{1,0:T(8,128)(2,1)S(1)} %get-tuple-element.72), channel_id=1, source_target_pairs={{0,1},{1,0},{2,3},{3,2},{4,5},{5,4},{6,7},{7,6},{8,9},{9,8},{10,11... | collective-permute-start | bytes 589832 | tf_op jit(solution)/shard_map/ppermute | solution.py:301
  79.0 8.6 %collective-permute-start.16 = (bf16[48,2048]{1,0:T(8,128)(2,1)S(1)}, bf16[48,2048]{1,0:T(8,128)(2,1)S(1)}, u32[]{:S(2)}, u32[]{:S(2)}) collective-permute-start(bf16[48,2048]{1,0:T(8,128)(2,1)S(1)} %get-tuple-element.73), channel_id=1, source_target_pairs={{0,9},{1,8},{2,11},{3,10},{4,13},{5,12},{6,15},{7,14},{8,1},{9,0},... | collective-permute-start | bytes 589832 | tf_op jit(solution)/shard_map/ppermute | solution.py:301
  79.7 10.5 %collective-permute-start.17 = (bf16[48,2048]{1,0:T(8,128)(2,1)S(1)}, bf16[48,2048]{1,0:T(8,128)(2,1)S(1)}, u32[]{:S(2)}, u32[]{:S(2)}) collective-permute-start(bf16[48,2048]{1,0:T(8,128)(2,1)S(1)} %get-tuple-element.74), channel_id=1, source_target_pairs={{0,17},{1,16},{2,19},{3,18},{4,21},{5,20},{6,23},{7,22},{8,25},{9,... | collective-permute-start | bytes 589832 | tf_op jit(solution)/shard_map/ppermute | solution.py:301
  82.3 8.4 %collective-permute-start.18 = (bf16[48,2048]{1,0:T(8,128)(2,1)S(1)}, bf16[48,2048]{1,0:T(8,128)(2,1)S(1)}, u32[]{:S(2)}, u32[]{:S(2)}) collective-permute-start(bf16[48,2048]{1,0:T(8,128)(2,1)S(1)} %get-tuple-element.75), channel_id=1, source_target_pairs={{0,25},{1,24},{2,27},{3,26},{4,29},{5,28},{6,31},{7,30},{8,17},{9,... | collective-permute-start | bytes 589832 | tf_op jit(solution)/shard_map/ppermute | solution.py:301
  82.6 8.1 %copy-start = (bf16[512,2048]{1,0:T(8,128)(2,1)S(1)}, bf16[512,2048]{1,0:T(8,128)(2,1)}, u32[]{:S(2)}) copy-start(bf16[512,2048]{1,0:T(8,128)(2,1)} %refs_11_.3) | copy-start | bytes 6291460
  85.6 9.1 %collective-permute-start.32 = (bf16[48,2048]{1,0:T(8,128)(2,1)S(1)}, bf16[48,2048]{1,0:T(8,128)(2,1)S(1)}, u32[]{:S(2)}, u32[]{:S(2)}) collective-permute-start(bf16[48,2048]{1,0:T(8,128)(2,1)S(1)} %get-tuple-element.93), channel_id=1, source_target_pairs={{0,8},{1,9},{2,10},{3,11},{4,12},{5,13},{6,14},{7,15},{8,0},{9,1},... | collective-permute-start | bytes 589832 | tf_op jit(solution)/shard_map/ppermute | solution.py:301
  87.1 11.4 %collective-permute-start.33 = (bf16[48,2048]{1,0:T(8,128)(2,1)S(1)}, bf16[48,2048]{1,0:T(8,128)(2,1)S(1)}, u32[]{:S(2)}, u32[]{:S(2)}) collective-permute-start(bf16[48,2048]{1,0:T(8,128)(2,1)S(1)} %get-tuple-element.94), channel_id=1, source_target_pairs={{0,16},{1,17},{2,18},{3,19},{4,20},{5,21},{6,22},{7,23},{8,24},{9,... | collective-permute-start | bytes 589832 | tf_op jit(solution)/shard_map/ppermute | solution.py:301
  87.6 12.9 %collective-permute-start.34 = (bf16[48,2048]{1,0:T(8,128)(2,1)S(1)}, bf16[48,2048]{1,0:T(8,128)(2,1)S(1)}, u32[]{:S(2)}, u32[]{:S(2)}) collective-permute-start(bf16[48,2048]{1,0:T(8,128)(2,1)S(1)} %get-tuple-element.95), channel_id=1, source_target_pairs={{0,24},{1,25},{2,26},{3,27},{4,28},{5,29},{6,30},{7,31},{8,16},{9,... | collective-permute-start | bytes 589832 | tf_op jit(solution)/shard_map/ppermute | solution.py:301
  91.4 26.3 %collective-permute-start.19 = (bf16[64,2048]{1,0:T(8,128)(2,1)S(1)}, bf16[64,2048]{1,0:T(8,128)(2,1)S(1)}, u32[]{:S(2)}, u32[]{:S(2)}) collective-permute-start(bf16[64,2048]{1,0:T(8,128)(2,1)S(1)} %get-tuple-element.80), channel_id=1, source_target_pairs={{2,0},{3,1},{4,6},{5,7},{10,8},{11,9},{12,14},{13,15},{18,16},{19,... | collective-permute-start | bytes 786440 | tf_op jit(solution)/shard_map/ppermute | solution.py:320
  92.7 9.5 %collective-permute-start.35 = (bf16[48,2048]{1,0:T(8,128)(2,1)S(1)}, bf16[48,2048]{1,0:T(8,128)(2,1)S(1)}, u32[]{:S(2)}, u32[]{:S(2)}) collective-permute-start(bf16[48,2048]{1,0:T(8,128)(2,1)S(1)} %get-tuple-element.96), channel_id=1, source_target_pairs={{0,1},{1,0},{2,3},{3,2},{4,5},{5,4},{6,7},{7,6},{8,9},{9,8},{10,11... | collective-permute-start | bytes 589832 | tf_op jit(solution)/shard_map/ppermute | solution.py:301
  94.6 8.8 %collective-permute-start.36 = (bf16[48,2048]{1,0:T(8,128)(2,1)S(1)}, bf16[48,2048]{1,0:T(8,128)(2,1)S(1)}, u32[]{:S(2)}, u32[]{:S(2)}) collective-permute-start(bf16[48,2048]{1,0:T(8,128)(2,1)S(1)} %get-tuple-element.97), channel_id=1, source_target_pairs={{0,9},{1,8},{2,11},{3,10},{4,13},{5,12},{6,15},{7,14},{8,1},{9,0},... | collective-permute-start | bytes 589832 | tf_op jit(solution)/shard_map/ppermute | solution.py:301
  98.6 11.4 %collective-permute-start.37 = (bf16[48,2048]{1,0:T(8,128)(2,1)S(1)}, bf16[48,2048]{1,0:T(8,128)(2,1)S(1)}, u32[]{:S(2)}, u32[]{:S(2)}) collective-permute-start(bf16[48,2048]{1,0:T(8,128)(2,1)S(1)} %get-tuple-element.98), channel_id=1, source_target_pairs={{0,17},{1,16},{2,19},{3,18},{4,21},{5,20},{6,23},{7,22},{8,25},{9,... | collective-permute-start | bytes 589832 | tf_op jit(solution)/shard_map/ppermute | solution.py:301
  100.6 9.4 %collective-permute-start.38 = (bf16[48,2048]{1,0:T(8,128)(2,1)S(1)}, bf16[48,2048]{1,0:T(8,128)(2,1)S(1)}, u32[]{:S(2)}, u32[]{:S(2)}) collective-permute-start(bf16[48,2048]{1,0:T(8,128)(2,1)S(1)} %get-tuple-element.99), channel_id=1, source_target_pairs={{0,25},{1,24},{2,27},{3,26},{4,29},{5,28},{6,31},{7,30},{8,17},{9,... | collective-permute-start | bytes 589832 | tf_op jit(solution)/shard_map/ppermute | solution.py:301
  102.1 16.5 %collective-permute-start.20 = (bf16[64,2048]{1,0:T(8,128)(2,1)S(1)}, bf16[64,2048]{1,0:T(8,128)(2,1)S(1)}, u32[]{:S(2)}, u32[]{:S(2)}) collective-permute-start(bf16[64,2048]{1,0:T(8,128)(2,1)S(1)} %get-tuple-element.81), channel_id=1, source_target_pairs={{4,0},{5,1},{2,6},{3,7},{12,8},{13,9},{10,14},{11,15},{20,16},{21,... | collective-permute-start | bytes 786440 | tf_op jit(solution)/shard_map/ppermute | solution.py:320
  103.4 15.2 %collective-permute-start.21 = (bf16[64,2048]{1,0:T(8,128)(2,1)S(1)}, bf16[64,2048]{1,0:T(8,128)(2,1)S(1)}, u32[]{:S(2)}, u32[]{:S(2)}) collective-permute-start(bf16[64,2048]{1,0:T(8,128)(2,1)S(1)} %get-tuple-element.82), channel_id=1, source_target_pairs={{6,0},{7,1},{0,6},{1,7},{14,8},{15,9},{8,14},{9,15},{22,16},{23,17... | collective-permute-start | bytes 786440 | tf_op jit(solution)/shard_map/ppermute | solution.py:320
  110.7 11.4 %collective-permute-start.39 = (bf16[64,2048]{1,0:T(8,128)(2,1)S(1)}, bf16[64,2048]{1,0:T(8,128)(2,1)S(1)}, u32[]{:S(2)}, u32[]{:S(2)}) collective-permute-start(bf16[64,2048]{1,0:T(8,128)(2,1)S(1)} %get-tuple-element.104), channel_id=1, source_target_pairs={{0,2},{1,3},{6,4},{7,5},{8,10},{9,11},{14,12},{15,13},{16,18},{17,... | collective-permute-start | bytes 786440 | tf_op jit(solution)/shard_map/ppermute | solution.py:320
  115.4 11.5 %collective-permute-start.40 = (bf16[64,2048]{1,0:T(8,128)(2,1)S(1)}, bf16[64,2048]{1,0:T(8,128)(2,1)S(1)}, u32[]{:S(2)}, u32[]{:S(2)}) collective-permute-start(bf16[64,2048]{1,0:T(8,128)(2,1)S(1)} %get-tuple-element.105), channel_id=1, source_target_pairs={{6,2},{7,3},{0,4},{1,5},{14,10},{15,11},{8,12},{9,13},{22,18},{23,... | collective-permute-start | bytes 786440 | tf_op jit(solution)/shard_map/ppermute | solution.py:320
  117.7 9.2 %collective-permute-start.41 = (bf16[64,2048]{1,0:T(8,128)(2,1)S(1)}, bf16[64,2048]{1,0:T(8,128)(2,1)S(1)}, u32[]{:S(2)}, u32[]{:S(2)}) collective-permute-start(bf16[64,2048]{1,0:T(8,128)(2,1)S(1)} %get-tuple-element.106), channel_id=1, source_target_pairs={{4,2},{5,3},{2,4},{3,5},{12,10},{13,11},{10,12},{11,13},{20,18},{2... | collective-permute-start | bytes 786440 | tf_op jit(solution)/shard_map/ppermute | solution.py:320
  (5 other events, 3.8 us)

commit v2 on v1

v2 whole, which is shorter than its diff:
```python
import functools

import jax
import jax.numpy as jnp
from jax import lax
from jax.experimental import pallas as pl
from jax.experimental.pallas import tpu as pltpu
from jax.sharding import PartitionSpec as P


ROUTED_SCALE = 2.5
EPSILON = 1e-05


F32 = jnp.float32
BF16 = jnp.bfloat16
VM = pl.BlockSpec(memory_space=pltpu.VMEM)
HB = pl.BlockSpec(memory_space=pltpu.HBM)
MIB = 1 << 20


def call(body, outs, operands, limit=16, scratch=(), specs=None):
    specs = specs or [VM] * len(operands)
    operands = [
        pltpu.with_memory_space_constraint(o, pltpu.HBM) if s is HB else o
        for o, s in zip(operands, specs)
    ]
    return pl.pallas_call(
        body,
        out_shape=outs,
        in_specs=specs,
        out_specs=jax.tree.map(lambda _: VM, outs),
        scratch_shapes=list(scratch),
        compiler_params=pltpu.CompilerParams(vmem_limit_bytes=limit * MIB),
    )(*operands)


def silu_times(gate, up):
    return (gate / (1.0 + jnp.exp(-gate)) * up).astype(BF16)


def route_body(block, cap, chunks, merged, ids_far, aff_far, *rest):
    ids, aff, arrived = rest[-3:]
    outs = rest[4:-7]
    moves = [
        pltpu.make_async_copy(source, target, arrived.at[n])
        for n, (source, target) in enumerate(
            zip((ids_far, aff_far) + rest[:4], (ids, aff) + rest[-7:-3])
        )
    ]
    for move in moves:
        move.start()
    hosts, levels = lax.axis_size("ep"), lax.axis_size("tp") // 2
    members = 2 * levels
    group, column = lax.axis_index("ep"), lax.axis_index("tp")
    core = lax.rem(column, 2)
    count = ids.shape[1]
    row = lax.broadcasted_iota(jnp.int32, (count, count), 0)
    col = lax.broadcasted_iota(jnp.int32, (count, count), 1)
    upper = jnp.where((row // block == col // block) & (row < col), 1.0, 0.0).astype(BF16)
    for move in moves[:2]:
        move.wait()
    here = ids[...]
    share = aff[...]
    share = share / jnp.sum(share, axis=0, keepdims=True) * ROUTED_SCALE
    marks, picked = [], []
    for s in range(2):
        for k in range(hosts):
            hit = here == (group ^ k) * members + (column ^ s)
            marks.append(jnp.max(jnp.where(hit, 1.0, 0.0), axis=0, keepdims=True))
            picked.append(jnp.sum(jnp.where(hit, share, 0.0), axis=0, keepdims=True))
    mark = jnp.concatenate(marks, axis=0)
    weight = jnp.concatenate(picked, axis=0)
    rank = jnp.dot(mark.astype(BF16), upper, preferred_element_type=F32).astype(jnp.int32)
    rank = jnp.where(mark > 0, rank, -count * count)

    def arranged(array, chunk, side):
        starts = [(2 * a + side) * block for a in chunk]
        return jnp.concatenate([array[:, n : n + block] for n in starts], axis=1)

    def placed(chunk, side):
        ranks = arranged(rank, chunk, side)
        return ranks + lax.broadcasted_iota(jnp.int32, ranks.shape, 1) // block * cap

    for q, chunk in enumerate(chunks):
        for side in range(2):
            ranks = placed(chunk, side)[:hosts] + side * len(chunk) * cap
            for n in range(len(chunk)):
                start = (2 * n + side) * block
                outs[q][:, start : start + block] = ranks[:, n * block : (n + 1) * block]
    for q, parts in enumerate(merged):
        chunk = sum([chunks[n] for n in parts], [])
        key, share = outs[len(chunks) + 2 * q : len(chunks) + 2 * q + 2]
        key[...] = jnp.where(core == 0, placed(chunk, 0), placed(chunk, 1))
        share[...] = jnp.where(core == 0, arranged(weight, chunk, 0), arranged(weight, chunk, 1))
    for move in moves[2:]:
        move.wait()


def norm_body(hosts, block, *refs):
    levels = lax.axis_size("tp") // 2
    column = lax.axis_index("tp")
    level, core = column // 2, lax.rem(column, 2)
    pieces = 2 * levels
    parts = refs[:pieces]
    gain, shift, key, gate_own, up_own, gate_other, up_other = refs[pieces : pieces + 7]
    slots = refs[pieces + 7 : pieces + 7 + hosts]
    hidden = refs[pieces + 7 + hosts]
    rows, width = parts[0].shape
    cap = slots[0].shape[1]
    scale = 1.0 / (pieces * width)
    mean = sum(jnp.sum(p[...].astype(F32), axis=1, keepdims=True) for p in parts) * scale
    spread = 0.0
    for p in parts:
        center = p[...].astype(F32) - mean
        spread = spread + jnp.sum(center * center, axis=1, keepdims=True)
    factor = lax.rsqrt(spread * scale + EPSILON)
    order = lax.broadcasted_iota(jnp.int32, (cap, rows), 0)
    pick = jnp.concatenate(
        [jnp.where(order == key[k : k + 1, :], 1.0, 0.0) for k in range(hosts)], axis=0
    ).astype(BF16)
    contract = (((1,), (1,)), ((), ()))
    acts = [0.0] * 4
    for n, p in enumerate(parts):
        at = 2 * (level ^ (n // 2)) + (core ^ (n % 2))
        span = pl.ds(pl.multiple_of(at * width, width), width)
        normed = (p[...].astype(F32) - mean) * factor * gain[:, span] + shift[:, span]
        normed = normed.astype(BF16)
        moved = jnp.dot(pick, normed, preferred_element_type=F32).astype(BF16)
        for k in range(hosts):
            slots[k][at] = moved[k * cap : (k + 1) * cap]
        sides = [
            jnp.concatenate(
                [normed[m : m + block] for m in range(s * block, rows, 2 * block)], axis=0
            )
            for s in range(2)
        ]
        owned = jnp.where(core == 0, *sides)
        for i, w in enumerate((gate_own, gate_other, up_own, up_other)):
            acts[i] = acts[i] + lax.dot_general(
                owned, w[:, span], contract, preferred_element_type=F32
            )
    gate = jnp.concatenate(acts[:2], axis=1)
    up = jnp.concatenate(acts[2:], axis=1)
    hidden[...] = silu_times(gate, up)


def expert_body(hosts, *refs):
    core = lax.rem(lax.axis_index("tp"), 2)
    w_gate, w_up, w_down, keep, give, rows, near_down, arrived = refs[-8:]
    sources = refs[:-8]
    fetch = pltpu.make_async_copy(w_down.at[0], near_down, arrived)
    fetch.start()
    start = 0
    spans = []
    for source in sources:
        pieces, cap, width = source.shape
        for n in range(pieces):
            rows[start : start + cap, n * width : (n + 1) * width] = source[n]
        spans.append((start, cap // 2))
        start += cap
    gate = jnp.dot(rows[...], w_gate[0], preferred_element_type=F32)
    up = jnp.dot(rows[...], w_up[0], preferred_element_type=F32)
    hidden = silu_times(gate, up)
    fetch.wait()
    result = jnp.dot(hidden, near_down[...], preferred_element_type=F32)
    for k in range(hosts):
        mine = [spans[n] for n in range(k, len(spans), hosts)]
        low = jnp.concatenate([result[n : n + half] for n, half in mine], axis=0)
        high = jnp.concatenate([result[n + half : n + 2 * half] for n, half in mine], axis=0)
        keep[k] = jnp.where(core == 0, low, high).astype(BF16)
        give[k] = jnp.where(core == 0, high, low).astype(BF16)


def merge_body(hosts, keep, got, *outs):
    half = keep.shape[1]
    for n, out in enumerate(outs):
        k, part = n % hosts, n // hosts
        width = out.shape[1]
        out[:half] = keep[k, :, part * width : (part + 1) * width]
        out[half:] = got[k, :, part * width : (part + 1) * width]


def combine_body(chunk, part, *refs):
    hosts, levels = lax.axis_size("ep"), lax.axis_size("tp") // 2
    column = lax.axis_index("tp")
    level = column // 2
    returned = refs[:hosts]
    key, weight, down = refs[hosts : hosts + 3]
    outs = refs[-1 - levels : -1]
    hidden = refs[hosts + 3 : -1 - levels]
    whole = refs[-1]
    cap = returned[0].shape[0] // 2
    count = key.shape[1]
    block, width = outs[0].shape
    order = lax.broadcasted_iota(jnp.int32, (cap, count), 0)
    mix = []
    for k in range(hosts):
        for n in (k, hosts + k):
            mix.append(jnp.where(order == key[n : n + 1, :], weight[n : n + 1, :], 0.0))
    mix = jnp.concatenate(mix, axis=0).astype(BF16)
    source = jnp.concatenate([r[...] for r in returned], axis=0)
    acts = jnp.concatenate([h[...] for h in hidden], axis=0)
    units = acts.shape[1] // 2
    span = slice(part * width, (part + 1) * width)
    near = down[pl.ds(pl.multiple_of(column * units, units), units), span]
    far = down[pl.ds(pl.multiple_of((column ^ 1) * units, units), units), span]
    whole[...] = lax.dot_general(
        mix, source, (((0,), (0,)), ((), ())), preferred_element_type=F32
    ) + jnp.dot(acts, jnp.concatenate([near, far], axis=0), preferred_element_type=F32)
    for k in range(levels):
        spot = sum(jnp.where((level ^ k) == a, n, 0) for n, a in enumerate(chunk))
        rows = whole[pl.ds(pl.multiple_of(spot * block, block), block), :]
        outs[k][...] = rows.astype(outs[k].dtype)


def final_body(owners, *refs):
    levels = lax.axis_size("tp") // 2
    level = lax.axis_index("tp") // 2
    out = refs[-1]
    start = 0
    for chunk, splits in owners:
        inside = functools.reduce(jnp.logical_or, [level == a for a in chunk])
        mine = refs[start : start + splits * levels]
        start += splits * levels

        @pl.when(inside)
        def _():
            width = out.shape[1] // splits
            for n in range(splits):
                parts = mine[n * levels : (n + 1) * levels]
                out[:, n * width : (n + 1) * width] = sum(
                    p[...].astype(F32) for p in parts
                ).astype(BF16)


def plan(levels):
    if levels % 4:
        return [list(range(levels))], [[0]], [1]
    edge = levels // 4
    outer = list(range(edge)), list(range(levels - edge, levels))
    return [*outer, list(range(edge, levels - edge))], [[0, 1], [2]], [1, 2]


def on_device(
    tokens,
    norm_gain,
    norm_shift,
    expert_ids,
    affinity,
    expert_gate,
    expert_up,
    expert_down,
    shared_gate,
    shared_up,
    shared_down,
):
    hosts = lax.axis_size("ep")
    members = lax.axis_size("tp")
    levels = members // 2
    count, width = tokens.shape
    top = expert_ids.shape[1]
    full = width * members
    block = count // members
    cap = max(1, 2 * block * top // (hosts * members))
    units = shared_gate.shape[0]

    chunks, merged, splits = plan(levels)
    shape = jax.ShapeDtypeStruct

    def along(k):
        return [(2 * a + s, 2 * (a ^ k) + s) for a in range(levels) for s in range(2)]

    swap = [(i, i ^ 1) for i in range(members)]

    def across(k):
        return [
            (g * members + i, (g ^ k) * members + i) for g in range(hosts) for i in range(members)
        ]

    ordered = [
        tokens[2 * block * chunk[0] : 2 * block * (chunk[-1] + 1)] for chunk in chunks
    ]
    level_parts = [
        [mine] + [lax.ppermute(mine, "tp", along(k)) for k in range(1, levels)]
        for mine in ordered
    ]
    gate_other = lax.ppermute(shared_gate, "tp", swap)
    up_other = lax.ppermute(shared_up, "tp", swap)
    route = [shape((hosts, m.shape[0]), jnp.int32) for m in ordered]
    for parts in merged:
        rows = sum(len(chunks[n]) for n in parts) * block
        route += [shape((2 * hosts, rows), jnp.int32), shape((2 * hosts, rows), F32)]
    params = [norm_gain.reshape(1, full), norm_shift.reshape(1, full), shared_gate, shared_up]
    route = call(
        functools.partial(route_body, block, cap, chunks, merged),
        route + [shape(p.shape, p.dtype) for p in params],
        [expert_ids.T, affinity.T] + params,
        scratch=[
            pltpu.VMEM((top, count), jnp.int32),
            pltpu.VMEM((top, count), F32),
            pltpu.SemaphoreType.DMA((6,)),
        ],
        specs=[HB] * 6,
    )
    gain, shift, gate_own, up_own = route[-4:]

    slots_of, hidden_of = [], []
    for q, chunk in enumerate(chunks):
        parts = []
        for n, part in enumerate(level_parts[q]):
            if n or q:
                after = hidden_of[q - 1] if q else route[0]
                part = lax.optimization_barrier((part, after))[0]
            parts += [part, lax.ppermute(part, "tp", swap)]
        out = call(
            functools.partial(norm_body, hosts, block),
            [shape((members, 2 * len(chunk) * cap, width), BF16) for _ in range(hosts)]
            + [shape((len(chunk) * block, 2 * units), BF16)],
            parts + [gain, shift, route[q], gate_own, up_own, gate_other, up_other],
        )
        slots_of.append(
            [out[0]]
            + [lax.ppermute(out[k], ("ep", "tp"), across(k)) for k in range(1, hosts)]
        )
        hidden_of.append(out[hosts])

    returned_of = []
    for q, parts in enumerate(merged):
        half = sum(len(chunks[n]) for n in parts) * cap
        keep, give = call(
            functools.partial(expert_body, hosts),
            [shape((hosts, half, full), BF16)] * 2,
            sum([slots_of[n] for n in parts], []) + [expert_gate, expert_up, expert_down],
            24,
            [
                pltpu.VMEM((hosts * 2 * half, full), BF16),
                pltpu.VMEM(expert_down.shape[1:], BF16),
                pltpu.SemaphoreType.DMA(()),
            ],
            [VM] * (hosts * len(parts) + 2) + [HB],
        )
        got = lax.ppermute(give, "tp", swap)
        out = call(
            functools.partial(merge_body, hosts),
            [shape((2 * half, full // splits[q]), BF16)]
            * (hosts * splits[q]),
            [keep, got],
        )
        returned_of.append(
            [
                [out[p * hosts]]
                + [
                    lax.ppermute(out[p * hosts + k], ("ep", "tp"), across(k))
                    for k in range(1, hosts)
                ]
                for p in range(splits[q])
            ]
        )

    sums, owners = [], []
    for q, parts in enumerate(merged):
        chunk = sum([chunks[n] for n in parts], [])
        owners.append((chunk, splits[q]))
        for p in range(splits[q]):
            part_width = full // splits[q]
            out = call(
                functools.partial(combine_body, chunk, p),
                [shape((block, part_width), F32)]
                + [shape((block, part_width), BF16) for _ in range(levels - 1)],
                returned_of[q][p]
                + [route[len(chunks) + 2 * q], route[len(chunks) + 2 * q + 1], shared_down]
                + [hidden_of[n] for n in parts],
                16,
                [pltpu.VMEM((len(chunk) * block, part_width), F32)],
            )
            sums.append(out[0])
            for k in range(1, levels):
                pairs = [(2 * (a ^ k) + s, 2 * a + s) for a in chunk for s in range(2)]
                sums.append(lax.ppermute(out[k], "tp", pairs))
    return call(functools.partial(final_body, owners), shape((block, full), BF16), sums)


def solution(mesh):
    placed = (
        P("ep", "tp"),
        P(),
        P(),
        P("ep", None),
        P("ep", None),
        P(("ep", "tp"), None, None),
        P(("ep", "tp"), None, None),
        P(("ep", "tp"), None, None),
        P("tp", None),
        P("tp", None),
        P(),
    )
    return jax.shard_map(
        on_device, mesh=mesh, in_specs=placed, out_specs=P(("ep", "tp"), None), check_vma=False
    )
```

time: 130 us -> 133 us (1.023)
  starting transfers between devices: 47.9 us -> 60.2 us
  local copies, waits for them, and re-layouts: 7.22 us -> 0.91 us
  waiting for transfers between devices: 60 us -> 55.1 us
  Pallas kernels: 12.3 us -> 14.1 us
    ppermute x6 -> x9, waiting for transfers between devices: 8.53 us -> 1.81 us  [on_device(): sums.append(lax.ppermute(out[k], 'tp', pairs))]
    unnamed x22 -> x8, local copies, waits for them, and re-layouts: 6.33 us -> 0.02 us
    ppermute x6 -> x9, starting transfers between devices: 14.3 us -> 19.1 us  [on_device(): sums.append(lax.ppermute(out[k], 'tp', pairs))]
    ppermute x20, waiting for transfers between devices: 35.3 us -> 39.9 us  [the longest x9 21.1 us: on_device(): lax.ppermute(out[k], ('ep', 'tp'), across(k))]
    ppermute x6 -> x9, starting transfers between devices: 10.2 us -> 13.6 us  [on_device(): lax.ppermute(mine, 'tp', along(k))]
    ppermute x20, starting transfers between devices: 21.8 us -> 24.7 us  [the longest x9 12.7 us: on_device(): lax.ppermute(out[p * hosts + k], ('ep', 'tp'), across(k))]
    pallas_call x8 -> x12, Pallas kernels: 12.3 us -> 14.1 us  [call(): pl.pallas_call(body, out_shape=outs, in_specs=specs, out_specs=jax.tree.m...]
    ppermute x6 -> x9, waiting for transfers between devices: 14.9 us -> 13.4 us  [on_device(): lax.ppermute(mine, 'tp', along(k))]
  transfers between devices with their start and end apart: 42 -> 52, of which waited for: 18 -> 15; matrix products, arithmetic and copies ran while one was open for 0% -> 1% of each run, Pallas kernels for 7% -> 10%
where the time goes in v2:
time: 133 us; the launch traced here: 131 us
  starting transfers between devices  60.2 us (45%)
  waiting for transfers between devices  55.1 us (41%)
  Pallas kernels  14.1 us (11%)
    ppermute x9, waiting for transfers between devices, on_device(): lax.ppermute(out[k], ('ep', 'tp'), across(k))  21.1 us
    ppermute x9, starting transfers between devices, on_device(): sums.append(lax.ppermute(out[k], 'tp', pairs))  19.1 us
    ppermute x9, waiting for transfers between devices, on_device(): lax.ppermute(out[p * hosts + k], ('ep', 'tp'), across(k))  18.8 us
    pallas_call x12, Pallas kernels, call(): pl.pallas_call(body, out_shape=outs, in_specs=specs, out_specs=jax.tree.m...  14.1 us
    ppermute x9, starting transfers between devices, on_device(): lax.ppermute(mine, 'tp', along(k))  13.6 us
    ppermute x9, waiting for transfers between devices, on_device(): lax.ppermute(mine, 'tp', along(k))  13.4 us
    ppermute x9, starting transfers between devices, on_device(): lax.ppermute(out[p * hosts + k], ('ep', 'tp'), across(k))  12.7 us
    ppermute x9, starting transfers between devices, on_device(): lax.ppermute(out[k], ('ep', 'tp'), across(k))  11.9 us
  transfers between devices with their start and end apart: 52, of which 15 were waited for; matrix products, arithmetic and copies ran while one was open for 1% of the time, Pallas kernels for 10%

profile of v2, /device:TPU:0, one launch (start us, length us, event | category | flops | bytes accessed | tf_op | source)
XLA Modules:
  0.0 130.7 jit_solution(9093272125944426607)
XLA Ops:
  0.6 0.9 fusion
  1.4 3.1 %collective-permute-start.1 = (bf16[128,256]{1,0:T(8,128)(2,1)S(1)}, bf16[128,256]{1,0:T(8,128)(2,1)S(1)}, u32[]{:S(2)}, u32[]{:S(2)}) collective-permute-start(bf16[128,256]{1,0:T(8,128)(2,1)S(1)} %get-tuple-element.136.refs_0_), channel_id=1, source_target_pairs={{0,2},{1,3},{2,0},{3,1},{4,6},{5,7},{6,4},{7,5},{8,10},{9,11},{10,... | collective-permute-start | bytes 196616 | tf_op jit(solution)/shard_map/ppermute | solution.py:285
  4.5 2.6 %collective-permute-start.3 = (bf16[128,256]{1,0:T(8,128)(2,1)S(1)}, bf16[128,256]{1,0:T(8,128)(2,1)S(1)}, u32[]{:S(2)}, u32[]{:S(2)}) collective-permute-start(bf16[128,256]{1,0:T(8,128)(2,1)S(1)} %get-tuple-element.136.refs_0_), channel_id=1, source_target_pairs={{0,4},{1,5},{2,6},{3,7},{4,0},{5,1},{6,2},{7,3},{8,12},{9,13},{10,... | collective-permute-start | bytes 196616 | tf_op jit(solution)/shard_map/ppermute | solution.py:285
  7.1 1.2 shard_map.109
  8.3 3.7 %collective-permute-done.3.refs_4_ = bf16[128,256]{1,0:T(8,128)(2,1)S(1)} collective-permute-done((bf16[128,256]{1,0:T(8,128)(2,1)S(1)}, bf16[128,256]{1,0:T(8,128)(2,1)S(1)}, u32[]{:S(2)}, u32[]{:S(2)}) %collective-permute-start.3) | collective-permute-done | bytes 65568 | tf_op jit(solution)/shard_map/ppermute | solution.py:285
  12.0 1.3 collective-permute-done.5.refs_6_
  14.5 2.5 %collective-permute-start.15 = (bf16[128,256]{1,0:T(8,128)(2,1)S(1)}, bf16[128,256]{1,0:T(8,128)(2,1)S(1)}, u32[]{:S(2)}, u32[]{:S(2)}) collective-permute-start(bf16[128,256]{1,0:T(8,128)(2,1)S(1)} %get-tuple-element.83.refs_0_), channel_id=1, source_target_pairs={{0,4},{1,5},{2,6},{3,7},{4,0},{5,1},{6,2},{7,3},{8,12},{9,13},{10,... | collective-permute-start | bytes 196616 | tf_op jit(solution)/shard_map/ppermute | solution.py:285
  17.0 1.2 collective-permute-start.17
  18.2 1.2 shard_map.110
  20.1 2.2 %collective-permute-done.15.refs_4_ = bf16[128,256]{1,0:T(8,128)(2,1)S(1)} collective-permute-done((bf16[128,256]{1,0:T(8,128)(2,1)S(1)}, bf16[128,256]{1,0:T(8,128)(2,1)S(1)}, u32[]{:S(2)}, u32[]{:S(2)}) %collective-permute-start.15) | collective-permute-done | bytes 65568 | tf_op jit(solution)/shard_map/ppermute | solution.py:285
  22.3 0.9 collective-permute-done.17.refs_6_
  23.2 1.9 %collective-permute-start.32 = (bf16[256,256]{1,0:T(8,128)(2,1)S(1)}, bf16[256,256]{1,0:T(8,128)(2,1)S(1)}, u32[]{:S(2)}, u32[]{:S(2)}) collective-permute-start(bf16[256,256]{1,0:T(8,128)(2,1)S(1)} %slice.11.refs_0_), channel_id=1, source_target_pairs={{0,4},{1,5},{2,6},{3,7},{4,0},{5,1},{6,2},{7,3},{8,12},{9,13},{10,... | collective-permute-start | bytes 393224 | tf_op jit(solution)/shard_map/ppermute | solution.py:285
  25.2 1.6 %collective-permute-start.34 = (bf16[256,256]{1,0:T(8,128)(2,1)S(1)}, bf16[256,256]{1,0:T(8,128)(2,1)S(1)}, u32[]{:S(2)}, u32[]{:S(2)}) collective-permute-start(bf16[256,256]{1,0:T(8,128)(2,1)S(1)} %slice.11.refs_0_), channel_id=1, source_target_pairs={{0,6},{1,7},{2,4},{3,5},{4,2},{5,3},{6,0},{7,1},{8,14},{9,15},{10,... | collective-permute-start | bytes 393224 | tf_op jit(solution)/shard_map/ppermute | solution.py:285
  26.7 1.6 %collective-permute-start.9 = (bf16[8,48,256]{2,1,0:T(8,128)(2,1)S(1)}, bf16[8,48,256]{2,1,0:T(8,128)(2,1)S(1)}, u32[]{:S(2)}, u32[]{:S(2)}) collective-permute-start(bf16[8,48,256]{2,1,0:T(8,128)(2,1)S(1)} %get-tuple-element.79), channel_id=1, source_target_pairs={{0,8},{1,9},{2,10},{3,11},{4,12},{5,13},{6,14},{7,15},{8,0},{9,1},... | collective-permute-start | bytes 589832 | tf_op jit(solution)/shard_map/ppermute | solution.py:324
  28.3 1.2 shard_map.111
  30.0 5.3 %collective-permute-done.32.refs_4_ = bf16[256,256]{1,0:T(8,128)(2,1)S(1)} collective-permute-done((bf16[256,256]{1,0:T(8,128)(2,1)S(1)}, bf16[256,256]{1,0:T(8,128)(2,1)S(1)}, u32[]{:S(2)}, u32[]{:S(2)}) %collective-permute-start.32) | collective-permute-done | bytes 131104 | tf_op jit(solution)/shard_map/ppermute | solution.py:285
  35.8 1.5 %collective-permute-start.10 = (bf16[8,48,256]{2,1,0:T(8,128)(2,1)S(1)}, bf16[8,48,256]{2,1,0:T(8,128)(2,1)S(1)}, u32[]{:S(2)}, u32[]{:S(2)}) collective-permute-start(bf16[8,48,256]{2,1,0:T(8,128)(2,1)S(1)} %get-tuple-element.80), channel_id=1, source_target_pairs={{0,16},{1,17},{2,18},{3,19},{4,20},{5,21},{6,22},{7,23},{8,24},{9,... | collective-permute-start | bytes 589832 | tf_op jit(solution)/shard_map/ppermute | solution.py:324
  37.4 1.4 %collective-permute-start.11 = (bf16[8,48,256]{2,1,0:T(8,128)(2,1)S(1)}, bf16[8,48,256]{2,1,0:T(8,128)(2,1)S(1)}, u32[]{:S(2)}, u32[]{:S(2)}) collective-permute-start(bf16[8,48,256]{2,1,0:T(8,128)(2,1)S(1)} %get-tuple-element.81), channel_id=1, source_target_pairs={{0,24},{1,25},{2,26},{3,27},{4,28},{5,29},{6,30},{7,31},{8,16},{9,... | collective-permute-start | bytes 589832 | tf_op jit(solution)/shard_map/ppermute | solution.py:324
  39.3 1.5 %collective-permute-start.20 = (bf16[8,48,256]{2,1,0:T(8,128)(2,1)S(1)}, bf16[8,48,256]{2,1,0:T(8,128)(2,1)S(1)}, u32[]{:S(2)}, u32[]{:S(2)}) collective-permute-start(bf16[8,48,256]{2,1,0:T(8,128)(2,1)S(1)} %get-tuple-element.90), channel_id=1, source_target_pairs={{0,16},{1,17},{2,18},{3,19},{4,20},{5,21},{6,22},{7,23},{8,24},{9,... | collective-permute-start | bytes 589832 | tf_op jit(solution)/shard_map/ppermute | solution.py:324
  40.9 1.4 %collective-permute-start.21 = (bf16[8,48,256]{2,1,0:T(8,128)(2,1)S(1)}, bf16[8,48,256]{2,1,0:T(8,128)(2,1)S(1)}, u32[]{:S(2)}, u32[]{:S(2)}) collective-permute-start(bf16[8,48,256]{2,1,0:T(8,128)(2,1)S(1)} %get-tuple-element.91), channel_id=1, source_target_pairs={{0,24},{1,25},{2,26},{3,27},{4,28},{5,29},{6,30},{7,31},{8,16},{9,... | collective-permute-start | bytes 589832 | tf_op jit(solution)/shard_map/ppermute | solution.py:324
  42.3 2.0 %shard_map.115 = (bf16[8,96,256]{2,1,0:T(8,128)(2,1)S(1)}, bf16[8,96,256]{2,1,0:T(8,128)(2,1)S(1)}, bf16[8,96,256]{2,1,0:T(8,128)(2,1)S(1)}, bf16[8,96,256]{2,1,0:T(8,128)(2,1)S(1)}, bf16[128,128]{1,0:T(8,128)(2,1)S(1)}) custom-call(bf16[256,256]{1,0:T(8,128)(2,1)S(1)} %slice.11.refs_0_, bf16[256,256]{1,0:T(8,128)(2,1)S(1)} %collective-permute-done.29.refs_1_, ...), custom_call_target="tpu_custom_call" | custom-call | tf_op jit(solution)/shard_map/pallas_call | solution.py:28
  44.3 3.5 %collective-permute-done.10.refs_2_ = bf16[8,48,256]{2,1,0:T(8,128)(2,1)S(1)} collective-permute-done((bf16[8,48,256]{2,1,0:T(8,128)(2,1)S(1)}, bf16[8,48,256]{2,1,0:T(8,128)(2,1)S(1)}, u32[]{:S(2)}, u32[]{:S(2)}) %collective-permute-start.10) | collective-permute-done | bytes 196640 | tf_op jit(solution)/shard_map/ppermute | solution.py:324
  47.8 1.5 %collective-permute-start.36 = (bf16[8,96,256]{2,1,0:T(8,128)(2,1)S(1)}, bf16[8,96,256]{2,1,0:T(8,128)(2,1)S(1)}, u32[]{:S(2)}, u32[]{:S(2)}) collective-permute-start(bf16[8,96,256]{2,1,0:T(8,128)(2,1)S(1)} %get-tuple-element.111), channel_id=1, source_target_pairs={{0,8},{1,9},{2,10},{3,11},{4,12},{5,13},{6,14},{7,15},{8,0},{9,1},... | collective-permute-start | bytes 1179656 | tf_op jit(solution)/shard_map/ppermute | solution.py:324
  49.3 2.4 %collective-permute-start.37 = (bf16[8,96,256]{2,1,0:T(8,128)(2,1)S(1)}, bf16[8,96,256]{2,1,0:T(8,128)(2,1)S(1)}, u32[]{:S(2)}, u32[]{:S(2)}) collective-permute-start(bf16[8,96,256]{2,1,0:T(8,128)(2,1)S(1)} %get-tuple-element.112), channel_id=1, source_target_pairs={{0,16},{1,17},{2,18},{3,19},{4,20},{5,21},{6,22},{7,23},{8,24},{9,... | collective-permute-start | bytes 1179656 | tf_op jit(solution)/shard_map/ppermute | solution.py:324
  51.8 4.5 %collective-permute-done.20.refs_6_ = bf16[8,48,256]{2,1,0:T(8,128)(2,1)S(1)} collective-permute-done((bf16[8,48,256]{2,1,0:T(8,128)(2,1)S(1)}, bf16[8,48,256]{2,1,0:T(8,128)(2,1)S(1)}, u32[]{:S(2)}, u32[]{:S(2)}) %collective-permute-start.20) | collective-permute-done | bytes 196640 | tf_op jit(solution)/shard_map/ppermute | solution.py:324
  56.3 2.8 %shard_map.112 = (bf16[4,48,2048]{2,1,0:T(8,128)(2,1)S(1)}, bf16[4,48,2048]{2,1,0:T(8,128)(2,1)S(1)}) custom-call(bf16[8,48,256]{2,1,0:T(8,128)(2,1)S(1)} %get-tuple-element.78.refs_0_, bf16[8,48,256]{2,1,0:T(8,128)(2,1)S(1)} %collective-permute-done.9.refs_1_, bf16[8,48,256]{2,1,0:T(8,128)(2,1)S(1)} %collective-permute-done.10.refs_2_, ...), custom_call_target="tpu_custom_call" | custom-call | tf_op jit(solution)/shard_map/pallas_call | solution.py:28
  59.2 2.8 %collective-permute-done.36.refs_1_ = bf16[8,96,256]{2,1,0:T(8,128)(2,1)S(1)} collective-permute-done((bf16[8,96,256]{2,1,0:T(8,128)(2,1)S(1)}, bf16[8,96,256]{2,1,0:T(8,128)(2,1)S(1)}, u32[]{:S(2)}, u32[]{:S(2)}) %collective-permute-start.36) | collective-permute-done | bytes 393248 | tf_op jit(solution)/shard_map/ppermute | solution.py:324
  62.0 10.2 %collective-permute-done.37.refs_2_ = bf16[8,96,256]{2,1,0:T(8,128)(2,1)S(1)} collective-permute-done((bf16[8,96,256]{2,1,0:T(8,128)(2,1)S(1)}, bf16[8,96,256]{2,1,0:T(8,128)(2,1)S(1)}, u32[]{:S(2)}, u32[]{:S(2)}) %collective-permute-start.37) | collective-permute-done | bytes 393248 | tf_op jit(solution)/shard_map/ppermute | solution.py:324
  72.2 3.3 %shard_map.116 = (bf16[4,48,2048]{2,1,0:T(8,128)(2,1)S(1)}, bf16[4,48,2048]{2,1,0:T(8,128)(2,1)S(1)}) custom-call(bf16[8,96,256]{2,1,0:T(8,128)(2,1)S(1)} %get-tuple-element.110.refs_0_, bf16[8,96,256]{2,1,0:T(8,128)(2,1)S(1)} %collective-permute-done.36.refs_1_, bf16[8,96,256]{2,1,0:T(8,128)(2,1)S(1)} %collective-permute-done.37.refs_2_, ...), custom_call_target="tpu_custom_call" | custom-call | tf_op jit(solution)/shard_map/pallas_call | solution.py:28
  75.7 1.6 %collective-permute-start.23 = (bf16[96,2048]{1,0:T(8,128)(2,1)S(1)}, bf16[96,2048]{1,0:T(8,128)(2,1)S(1)}, u32[]{:S(2)}, u32[]{:S(2)}) collective-permute-start(bf16[96,2048]{1,0:T(8,128)(2,1)S(1)} %get-tuple-element.95), channel_id=1, source_target_pairs={{0,8},{1,9},{2,10},{3,11},{4,12},{5,13},{6,14},{7,15},{8,0},{9,1},... | collective-permute-start | bytes 1179656 | tf_op jit(solution)/shard_map/ppermute | solution.py:354
  77.2 1.5 %collective-permute-start.24 = (bf16[96,2048]{1,0:T(8,128)(2,1)S(1)}, bf16[96,2048]{1,0:T(8,128)(2,1)S(1)}, u32[]{:S(2)}, u32[]{:S(2)}) collective-permute-start(bf16[96,2048]{1,0:T(8,128)(2,1)S(1)} %get-tuple-element.96), channel_id=1, source_target_pairs={{0,16},{1,17},{2,18},{3,19},{4,20},{5,21},{6,22},{7,23},{8,24},{9,... | collective-permute-start | bytes 1179656 | tf_op jit(solution)/shard_map/ppermute | solution.py:354
  79.4 1.6 %collective-permute-start.40 = (bf16[96,1024]{1,0:T(8,128)(2,1)S(1)}, bf16[96,1024]{1,0:T(8,128)(2,1)S(1)}, u32[]{:S(2)}, u32[]{:S(2)}) collective-permute-start(bf16[96,1024]{1,0:T(8,128)(2,1)S(1)} %get-tuple-element.117), channel_id=1, source_target_pairs={{0,8},{1,9},{2,10},{3,11},{4,12},{5,13},{6,14},{7,15},{8,0},{9,1},... | collective-permute-start | bytes 589832 | tf_op jit(solution)/shard_map/ppermute | solution.py:354
  80.9 1.5 %collective-permute-start.41 = (bf16[96,1024]{1,0:T(8,128)(2,1)S(1)}, bf16[96,1024]{1,0:T(8,128)(2,1)S(1)}, u32[]{:S(2)}, u32[]{:S(2)}) collective-permute-start(bf16[96,1024]{1,0:T(8,128)(2,1)S(1)} %get-tuple-element.118), channel_id=1, source_target_pairs={{0,16},{1,17},{2,18},{3,19},{4,20},{5,21},{6,22},{7,23},{8,24},{9,... | collective-permute-start | bytes 589832 | tf_op jit(solution)/shard_map/ppermute | solution.py:354
  82.4 5.3 %collective-permute-done.23.refs_1_ = bf16[96,2048]{1,0:T(8,128)(2,1)S(1)} collective-permute-done((bf16[96,2048]{1,0:T(8,128)(2,1)S(1)}, bf16[96,2048]{1,0:T(8,128)(2,1)S(1)}, u32[]{:S(2)}, u32[]{:S(2)}) %collective-permute-start.23) | collective-permute-done | bytes 393248 | tf_op jit(solution)/shard_map/ppermute | solution.py:354
  87.7 2.4 %collective-permute-start.42 = (bf16[96,1024]{1,0:T(8,128)(2,1)S(1)}, bf16[96,1024]{1,0:T(8,128)(2,1)S(1)}, u32[]{:S(2)}, u32[]{:S(2)}) collective-permute-start(bf16[96,1024]{1,0:T(8,128)(2,1)S(1)} %get-tuple-element.119), channel_id=1, source_target_pairs={{0,24},{1,25},{2,26},{3,27},{4,28},{5,29},{6,30},{7,31},{8,16},{9,... | collective-permute-start | bytes 589832 | tf_op jit(solution)/shard_map/ppermute | solution.py:354
  90.2 7.5 %collective-permute-done.24.refs_2_ = bf16[96,2048]{1,0:T(8,128)(2,1)S(1)} collective-permute-done((bf16[96,2048]{1,0:T(8,128)(2,1)S(1)}, bf16[96,2048]{1,0:T(8,128)(2,1)S(1)}, u32[]{:S(2)}, u32[]{:S(2)}) %collective-permute-start.24) | collective-permute-done | bytes 393248 | tf_op jit(solution)/shard_map/ppermute | solution.py:354
  97.7 2.1 %collective-permute-start.47 = (bf16[96,1024]{1,0:T(8,128)(2,1)S(1)}, bf16[96,1024]{1,0:T(8,128)(2,1)S(1)}, u32[]{:S(2)}, u32[]{:S(2)}) collective-permute-start(bf16[96,1024]{1,0:T(8,128)(2,1)S(1)} %get-tuple-element.129), channel_id=1, source_target_pairs={{0,16},{1,17},{2,18},{3,19},{4,20},{5,21},{6,22},{7,23},{8,24},{9,... | collective-permute-start | bytes 589832 | tf_op jit(solution)/shard_map/ppermute | solution.py:354
  100.4 1.3 collective-permute-start.26
  101.7 4.3 %collective-permute-done.41.refs_2_ = bf16[96,1024]{1,0:T(8,128)(2,1)S(1)} collective-permute-done((bf16[96,1024]{1,0:T(8,128)(2,1)S(1)}, bf16[96,1024]{1,0:T(8,128)(2,1)S(1)}, u32[]{:S(2)}, u32[]{:S(2)}) %collective-permute-start.41) | collective-permute-done | bytes 196640 | tf_op jit(solution)/shard_map/ppermute | solution.py:354
  106.1 1.3 collective-permute-start.27
  107.4 3.5 %collective-permute-start.28 = (bf16[64,2048]{1,0:T(8,128)(2,1)S(1)}, bf16[64,2048]{1,0:T(8,128)(2,1)S(1)}, u32[]{:S(2)}, u32[]{:S(2)}) collective-permute-start(bf16[64,2048]{1,0:T(8,128)(2,1)S(1)} %get-tuple-element.104), channel_id=1, source_target_pairs={{6,0},{7,1},{0,6},{1,7},{14,8},{15,9},{8,14},{9,15},{22,16},{23,17... | collective-permute-start | bytes 786440 | tf_op jit(solution)/shard_map/ppermute | solution.py:380
  110.9 1.6 %collective-permute-start.48 = (bf16[96,1024]{1,0:T(8,128)(2,1)S(1)}, bf16[96,1024]{1,0:T(8,128)(2,1)S(1)}, u32[]{:S(2)}, u32[]{:S(2)}) collective-permute-start(bf16[96,1024]{1,0:T(8,128)(2,1)S(1)} %get-tuple-element.130), channel_id=1, source_target_pairs={{0,24},{1,25},{2,26},{3,27},{4,28},{5,29},{6,30},{7,31},{8,16},{9,... | collective-permute-start | bytes 589832 | tf_op jit(solution)/shard_map/ppermute | solution.py:354
  112.9 3.0 %collective-permute-start.43 = (bf16[64,1024]{1,0:T(8,128)(2,1)S(1)}, bf16[64,1024]{1,0:T(8,128)(2,1)S(1)}, u32[]{:S(2)}, u32[]{:S(2)}) collective-permute-start(bf16[64,1024]{1,0:T(8,128)(2,1)S(1)} %get-tuple-element.124), channel_id=1, source_target_pairs={{0,2},{1,3},{6,4},{7,5},{8,10},{9,11},{14,12},{15,13},{16,18},{17,... | collective-permute-start | bytes 393224 | tf_op jit(solution)/shard_map/ppermute | solution.py:380
  115.9 1.6 %collective-permute-done.48.refs_3_ = bf16[96,1024]{1,0:T(8,128)(2,1)S(1)} collective-permute-done((bf16[96,1024]{1,0:T(8,128)(2,1)S(1)}, bf16[96,1024]{1,0:T(8,128)(2,1)S(1)}, u32[]{:S(2)}, u32[]{:S(2)}) %collective-permute-start.48) | collective-permute-done | bytes 196640 | tf_op jit(solution)/shard_map/ppermute | solution.py:354
  117.5 3.5 %collective-permute-start.44 = (bf16[64,1024]{1,0:T(8,128)(2,1)S(1)}, bf16[64,1024]{1,0:T(8,128)(2,1)S(1)}, u32[]{:S(2)}, u32[]{:S(2)}) collective-permute-start(bf16[64,1024]{1,0:T(8,128)(2,1)S(1)} %get-tuple-element.125), channel_id=1, source_target_pairs={{6,2},{7,3},{0,4},{1,5},{14,10},{15,11},{8,12},{9,13},{22,18},{23,... | collective-permute-start | bytes 393224 | tf_op jit(solution)/shard_map/ppermute | solution.py:380
  122.2 3.7 %collective-permute-start.49 = (bf16[64,1024]{1,0:T(8,128)(2,1)S(1)}, bf16[64,1024]{1,0:T(8,128)(2,1)S(1)}, u32[]{:S(2)}, u32[]{:S(2)}) collective-permute-start(bf16[64,1024]{1,0:T(8,128)(2,1)S(1)} %get-tuple-element.132), channel_id=1, source_target_pairs={{0,2},{1,3},{6,4},{7,5},{8,10},{9,11},{14,12},{15,13},{16,18},{17,... | collective-permute-start | bytes 393224 | tf_op jit(solution)/shard_map/ppermute | solution.py:380
  125.9 1.5 %collective-permute-start.50 = (bf16[64,1024]{1,0:T(8,128)(2,1)S(1)}, bf16[64,1024]{1,0:T(8,128)(2,1)S(1)}, u32[]{:S(2)}, u32[]{:S(2)}) collective-permute-start(bf16[64,1024]{1,0:T(8,128)(2,1)S(1)} %get-tuple-element.133), channel_id=1, source_target_pairs={{6,2},{7,3},{0,4},{1,5},{14,10},{15,11},{8,12},{9,13},{22,18},{23,... | collective-permute-start | bytes 393224 | tf_op jit(solution)/shard_map/ppermute | solution.py:380
  128.4 1.5 %collective-permute-done.50.refs_10_ = bf16[64,1024]{1,0:T(8,128)(2,1)S(1)} collective-permute-done((bf16[64,1024]{1,0:T(8,128)(2,1)S(1)}, bf16[64,1024]{1,0:T(8,128)(2,1)S(1)}, u32[]{:S(2)}, u32[]{:S(2)}) %collective-permute-start.50) | collective-permute-done | bytes 131104 | tf_op jit(solution)/shard_map/ppermute | solution.py:380
  (78 shorter events, 9.1 us)
Async XLA Ops:
  0.0 18.2 %collective-permute-start.7 = (bf16[64,2048]{1,0:T(8,128)(2,1)}, bf16[64,2048]{1,0:T(8,128)(2,1)S(1)}, u32[]{:S(2)}, u32[]{:S(2)}) collective-permute-start(bf16[64,2048]{1,0:T(8,128)(2,1)} %rest_2_.1), channel_id=1, source_target_pairs={{0,1},{1,0},{2,3},{3,2},{4,5},{5,4},{6,7},{7,6},{8,9},{9,8},{10,11... | collective-permute-start | bytes 786440 | tf_op jit(solution)/shard_map/ppermute | solution.py:288
  0.5 17.7 %collective-permute-start.8 = (bf16[64,2048]{1,0:T(8,128)(2,1)}, bf16[64,2048]{1,0:T(8,128)(2,1)S(1)}, u32[]{:S(2)}, u32[]{:S(2)}) collective-permute-start(bf16[64,2048]{1,0:T(8,128)(2,1)} %rest_3_.1), channel_id=1, source_target_pairs={{0,1},{1,0},{2,3},{3,2},{4,5},{5,4},{6,7},{7,6},{8,9},{9,8},{10,11... | collective-permute-start | bytes 786440 | tf_op jit(solution)/shard_map/ppermute | solution.py:289
  1.4 5.7 %collective-permute-start.1 = (bf16[128,256]{1,0:T(8,128)(2,1)S(1)}, bf16[128,256]{1,0:T(8,128)(2,1)S(1)}, u32[]{:S(2)}, u32[]{:S(2)}) collective-permute-start(bf16[128,256]{1,0:T(8,128)(2,1)S(1)} %get-tuple-element.136.refs_0_), channel_id=1, source_target_pairs={{0,2},{1,3},{2,0},{3,1},{4,6},{5,7},{6,4},{7,5},{8,10},{9,11},{10,... | collective-permute-start | bytes 196616 | tf_op jit(solution)/shard_map/ppermute | solution.py:285
  4.5 7.5 %collective-permute-start.3 = (bf16[128,256]{1,0:T(8,128)(2,1)S(1)}, bf16[128,256]{1,0:T(8,128)(2,1)S(1)}, u32[]{:S(2)}, u32[]{:S(2)}) collective-permute-start(bf16[128,256]{1,0:T(8,128)(2,1)S(1)} %get-tuple-element.136.refs_0_), channel_id=1, source_target_pairs={{0,4},{1,5},{2,6},{3,7},{4,0},{5,1},{6,2},{7,3},{8,12},{9,13},{10,... | collective-permute-start | bytes 196616 | tf_op jit(solution)/shard_map/ppermute | solution.py:285
  7.1 6.2 %collective-permute-start.5 = (bf16[128,256]{1,0:T(8,128)(2,1)S(1)}, bf16[128,256]{1,0:T(8,128)(2,1)S(1)}, u32[]{:S(2)}, u32[]{:S(2)}) collective-permute-start(bf16[128,256]{1,0:T(8,128)(2,1)S(1)} %get-tuple-element.136.refs_0_), channel_id=1, source_target_pairs={{0,6},{1,7},{2,4},{3,5},{4,2},{5,3},{6,0},{7,1},{8,14},{9,15},{10,... | collective-permute-start | bytes 196616 | tf_op jit(solution)/shard_map/ppermute | solution.py:285
  7.1 6.2 %collective-permute-start = (bf16[128,256]{1,0:T(8,128)(2,1)S(1)}, bf16[128,256]{1,0:T(8,128)(2,1)S(1)}, u32[]{:S(2)}, u32[]{:S(2)}) collective-permute-start(bf16[128,256]{1,0:T(8,128)(2,1)S(1)} %get-tuple-element.136.refs_0_), channel_id=1, source_target_pairs={{0,1},{1,0},{2,3},{3,2},{4,5},{5,4},{6,7},{7,6},{8,9},{9,8},{10,11... | collective-permute-start | bytes 196616 | tf_op jit(solution)/shard_map/ppermute | solution.py:315
  13.3 3.7 %collective-permute-start.6 = (bf16[128,256]{1,0:T(8,128)(2,1)S(1)}, bf16[128,256]{1,0:T(8,128)(2,1)S(1)}, u32[]{:S(2)}, u32[]{:S(2)}) collective-permute-start(bf16[128,256]{1,0:T(8,128)(2,1)S(1)} %collective-permute-done.5.refs_6_), channel_id=1, source_target_pairs={{0,1},{1,0},{2,3},{3,2},{4,5},{5,4},{6,7},{7,6},{8,9},{9,8},{10,11... | collective-permute-start | bytes 196616 | tf_op jit(solution)/shard_map/ppermute | solution.py:315
  13.8 5.7 %collective-permute-start.13 = (bf16[128,256]{1,0:T(8,128)(2,1)S(1)}, bf16[128,256]{1,0:T(8,128)(2,1)S(1)}, u32[]{:S(2)}, u32[]{:S(2)}) collective-permute-start(bf16[128,256]{1,0:T(8,128)(2,1)S(1)} %get-tuple-element.83.refs_0_), channel_id=1, source_target_pairs={{0,2},{1,3},{2,0},{3,1},{4,6},{5,7},{6,4},{7,5},{8,10},{9,11},{10,... | collective-permute-start | bytes 196616 | tf_op jit(solution)/shard_map/ppermute | solution.py:285
  14.5 7.7 %collective-permute-start.15 = (bf16[128,256]{1,0:T(8,128)(2,1)S(1)}, bf16[128,256]{1,0:T(8,128)(2,1)S(1)}, u32[]{:S(2)}, u32[]{:S(2)}) collective-permute-start(bf16[128,256]{1,0:T(8,128)(2,1)S(1)} %get-tuple-element.83.refs_0_), channel_id=1, source_target_pairs={{0,4},{1,5},{2,6},{3,7},{4,0},{5,1},{6,2},{7,3},{8,12},{9,13},{10,... | collective-permute-start | bytes 196616 | tf_op jit(solution)/shard_map/ppermute | solution.py:285
  17.0 6.2 %collective-permute-start.17 = (bf16[128,256]{1,0:T(8,128)(2,1)S(1)}, bf16[128,256]{1,0:T(8,128)(2,1)S(1)}, u32[]{:S(2)}, u32[]{:S(2)}) collective-permute-start(bf16[128,256]{1,0:T(8,128)(2,1)S(1)} %get-tuple-element.83.refs_0_), channel_id=1, source_target_pairs={{0,6},{1,7},{2,4},{3,5},{4,2},{5,3},{6,0},{7,1},{8,14},{9,15},{10,... | collective-permute-start | bytes 196616 | tf_op jit(solution)/shard_map/ppermute | solution.py:285
  19.4 5.8 %collective-permute-start.12 = (bf16[128,256]{1,0:T(8,128)(2,1)S(1)}, bf16[128,256]{1,0:T(8,128)(2,1)S(1)}, u32[]{:S(2)}, u32[]{:S(2)}) collective-permute-start(bf16[128,256]{1,0:T(8,128)(2,1)S(1)} %get-tuple-element.83.refs_0_), channel_id=1, source_target_pairs={{0,1},{1,0},{2,3},{3,2},{4,5},{5,4},{6,7},{7,6},{8,9},{9,8},{10,11... | collective-permute-start | bytes 196616 | tf_op jit(solution)/shard_map/ppermute | solution.py:315
  19.5 7.2 %collective-permute-start.14 = (bf16[128,256]{1,0:T(8,128)(2,1)S(1)}, bf16[128,256]{1,0:T(8,128)(2,1)S(1)}, u32[]{:S(2)}, u32[]{:S(2)}) collective-permute-start(bf16[128,256]{1,0:T(8,128)(2,1)S(1)} %collective-permute-done.13.refs_2_), channel_id=1, source_target_pairs={{0,1},{1,0},{2,3},{3,2},{4,5},{5,4},{6,7},{7,6},{8,9},{9,8},{10,11... | collective-permute-start | bytes 196616 | tf_op jit(solution)/shard_map/ppermute | solution.py:315
  20.0 9.7 %collective-permute-start.30 = (bf16[256,256]{1,0:T(8,128)(2,1)S(1)}, bf16[256,256]{1,0:T(8,128)(2,1)S(1)}, u32[]{:S(2)}, u32[]{:S(2)}) collective-permute-start(bf16[256,256]{1,0:T(8,128)(2,1)S(1)} %slice.11.refs_0_), channel_id=1, source_target_pairs={{0,2},{1,3},{2,0},{3,1},{4,6},{5,7},{6,4},{7,5},{8,10},{9,11},{10,... | collective-permute-start | bytes 393224 | tf_op jit(solution)/shard_map/ppermute | solution.py:285
  22.3 4.4 %collective-permute-start.16 = (bf16[128,256]{1,0:T(8,128)(2,1)S(1)}, bf16[128,256]{1,0:T(8,128)(2,1)S(1)}, u32[]{:S(2)}, u32[]{:S(2)}) collective-permute-start(bf16[128,256]{1,0:T(8,128)(2,1)S(1)} %collective-permute-done.15.refs_4_), channel_id=1, source_target_pairs={{0,1},{1,0},{2,3},{3,2},{4,5},{5,4},{6,7},{7,6},{8,9},{9,8},{10,11... | collective-permute-start | bytes 196616 | tf_op jit(solution)/shard_map/ppermute | solution.py:315
  23.2 12.1 %collective-permute-start.32 = (bf16[256,256]{1,0:T(8,128)(2,1)S(1)}, bf16[256,256]{1,0:T(8,128)(2,1)S(1)}, u32[]{:S(2)}, u32[]{:S(2)}) collective-permute-start(bf16[256,256]{1,0:T(8,128)(2,1)S(1)} %slice.11.refs_0_), channel_id=1, source_target_pairs={{0,4},{1,5},{2,6},{3,7},{4,0},{5,1},{6,2},{7,3},{8,12},{9,13},{10,... | collective-permute-start | bytes 393224 | tf_op jit(solution)/shard_map/ppermute | solution.py:285
  25.2 10.2 %collective-permute-start.34 = (bf16[256,256]{1,0:T(8,128)(2,1)S(1)}, bf16[256,256]{1,0:T(8,128)(2,1)S(1)}, u32[]{:S(2)}, u32[]{:S(2)}) collective-permute-start(bf16[256,256]{1,0:T(8,128)(2,1)S(1)} %slice.11.refs_0_), channel_id=1, source_target_pairs={{0,6},{1,7},{2,4},{3,5},{4,2},{5,3},{6,0},{7,1},{8,14},{9,15},{10,... | collective-permute-start | bytes 393224 | tf_op jit(solution)/shard_map/ppermute | solution.py:285
  26.7 9.1 %collective-permute-start.9 = (bf16[8,48,256]{2,1,0:T(8,128)(2,1)S(1)}, bf16[8,48,256]{2,1,0:T(8,128)(2,1)S(1)}, u32[]{:S(2)}, u32[]{:S(2)}) collective-permute-start(bf16[8,48,256]{2,1,0:T(8,128)(2,1)S(1)} %get-tuple-element.79), channel_id=1, source_target_pairs={{0,8},{1,9},{2,10},{3,11},{4,12},{5,13},{6,14},{7,15},{8,0},{9,1},... | collective-permute-start | bytes 589832 | tf_op jit(solution)/shard_map/ppermute | solution.py:324
  29.5 7.9 %collective-permute-start.29 = (bf16[256,256]{1,0:T(8,128)(2,1)S(1)}, bf16[256,256]{1,0:T(8,128)(2,1)S(1)}, u32[]{:S(2)}, u32[]{:S(2)}) collective-permute-start(bf16[256,256]{1,0:T(8,128)(2,1)S(1)} %slice.11.refs_0_), channel_id=1, source_target_pairs={{0,1},{1,0},{2,3},{3,2},{4,5},{5,4},{6,7},{7,6},{8,9},{9,8},{10,11... | collective-permute-start | bytes 393224 | tf_op jit(solution)/shard_map/ppermute | solution.py:315
  29.7 9.1 %collective-permute-start.31 = (bf16[256,256]{1,0:T(8,128)(2,1)S(1)}, bf16[256,256]{1,0:T(8,128)(2,1)S(1)}, u32[]{:S(2)}, u32[]{:S(2)}) collective-permute-start(bf16[256,256]{1,0:T(8,128)(2,1)S(1)} %collective-permute-done.30.refs_2_), channel_id=1, source_target_pairs={{0,1},{1,0},{2,3},{3,2},{4,5},{5,4},{6,7},{7,6},{8,9},{9,8},{10,11... | collective-permute-start | bytes 393224 | tf_op jit(solution)/shard_map/ppermute | solution.py:315
  35.3 4.0 %collective-permute-start.33 = (bf16[256,256]{1,0:T(8,128)(2,1)S(1)}, bf16[256,256]{1,0:T(8,128)(2,1)S(1)}, u32[]{:S(2)}, u32[]{:S(2)}) collective-permute-start(bf16[256,256]{1,0:T(8,128)(2,1)S(1)} %collective-permute-done.32.refs_4_), channel_id=1, source_target_pairs={{0,1},{1,0},{2,3},{3,2},{4,5},{5,4},{6,7},{7,6},{8,9},{9,8},{10,11... | collective-permute-start | bytes 393224 | tf_op jit(solution)/shard_map/ppermute | solution.py:315
  35.3 5.5 %collective-permute-start.35 = (bf16[256,256]{1,0:T(8,128)(2,1)S(1)}, bf16[256,256]{1,0:T(8,128)(2,1)S(1)}, u32[]{:S(2)}, u32[]{:S(2)}) collective-permute-start(bf16[256,256]{1,0:T(8,128)(2,1)S(1)} %collective-permute-done.34.refs_6_), channel_id=1, source_target_pairs={{0,1},{1,0},{2,3},{3,2},{4,5},{5,4},{6,7},{7,6},{8,9},{9,8},{10,11... | collective-permute-start | bytes 393224 | tf_op jit(solution)/shard_map/ppermute | solution.py:315
  35.8 12.0 %collective-permute-start.10 = (bf16[8,48,256]{2,1,0:T(8,128)(2,1)S(1)}, bf16[8,48,256]{2,1,0:T(8,128)(2,1)S(1)}, u32[]{:S(2)}, u32[]{:S(2)}) collective-permute-start(bf16[8,48,256]{2,1,0:T(8,128)(2,1)S(1)} %get-tuple-element.80), channel_id=1, source_target_pairs={{0,16},{1,17},{2,18},{3,19},{4,20},{5,21},{6,22},{7,23},{8,24},{9,... | collective-permute-start | bytes 589832 | tf_op jit(solution)/shard_map/ppermute | solution.py:324
  37.4 12.0 %collective-permute-start.11 = (bf16[8,48,256]{2,1,0:T(8,128)(2,1)S(1)}, bf16[8,48,256]{2,1,0:T(8,128)(2,1)S(1)}, u32[]{:S(2)}, u32[]{:S(2)}) collective-permute-start(bf16[8,48,256]{2,1,0:T(8,128)(2,1)S(1)} %get-tuple-element.81), channel_id=1, source_target_pairs={{0,24},{1,25},{2,26},{3,27},{4,28},{5,29},{6,30},{7,31},{8,16},{9,... | collective-permute-start | bytes 589832 | tf_op jit(solution)/shard_map/ppermute | solution.py:324
  38.8 12.9 %collective-permute-start.19 = (bf16[8,48,256]{2,1,0:T(8,128)(2,1)S(1)}, bf16[8,48,256]{2,1,0:T(8,128)(2,1)S(1)}, u32[]{:S(2)}, u32[]{:S(2)}) collective-permute-start(bf16[8,48,256]{2,1,0:T(8,128)(2,1)S(1)} %get-tuple-element.89), channel_id=1, source_target_pairs={{0,8},{1,9},{2,10},{3,11},{4,12},{5,13},{6,14},{7,15},{8,0},{9,1},... | collective-permute-start | bytes 589832 | tf_op jit(solution)/shard_map/ppermute | solution.py:324
  39.3 16.9 %collective-permute-start.20 = (bf16[8,48,256]{2,1,0:T(8,128)(2,1)S(1)}, bf16[8,48,256]{2,1,0:T(8,128)(2,1)S(1)}, u32[]{:S(2)}, u32[]{:S(2)}) collective-permute-start(bf16[8,48,256]{2,1,0:T(8,128)(2,1)S(1)} %get-tuple-element.90), channel_id=1, source_target_pairs={{0,16},{1,17},{2,18},{3,19},{4,20},{5,21},{6,22},{7,23},{8,24},{9,... | collective-permute-start | bytes 589832 | tf_op jit(solution)/shard_map/ppermute | solution.py:324
  40.9 15.4 %collective-permute-start.21 = (bf16[8,48,256]{2,1,0:T(8,128)(2,1)S(1)}, bf16[8,48,256]{2,1,0:T(8,128)(2,1)S(1)}, u32[]{:S(2)}, u32[]{:S(2)}) collective-permute-start(bf16[8,48,256]{2,1,0:T(8,128)(2,1)S(1)} %get-tuple-element.91), channel_id=1, source_target_pairs={{0,24},{1,25},{2,26},{3,27},{4,28},{5,29},{6,30},{7,31},{8,16},{9,... | collective-permute-start | bytes 589832 | tf_op jit(solution)/shard_map/ppermute | solution.py:324
  47.8 14.2 %collective-permute-start.36 = (bf16[8,96,256]{2,1,0:T(8,128)(2,1)S(1)}, bf16[8,96,256]{2,1,0:T(8,128)(2,1)S(1)}, u32[]{:S(2)}, u32[]{:S(2)}) collective-permute-start(bf16[8,96,256]{2,1,0:T(8,128)(2,1)S(1)} %get-tuple-element.111), channel_id=1, source_target_pairs={{0,8},{1,9},{2,10},{3,11},{4,12},{5,13},{6,14},{7,15},{8,0},{9,1},... | collective-permute-start | bytes 1179656 | tf_op jit(solution)/shard_map/ppermute | solution.py:324
  49.3 22.9 %collective-permute-start.37 = (bf16[8,96,256]{2,1,0:T(8,128)(2,1)S(1)}, bf16[8,96,256]{2,1,0:T(8,128)(2,1)S(1)}, u32[]{:S(2)}, u32[]{:S(2)}) collective-permute-start(bf16[8,96,256]{2,1,0:T(8,128)(2,1)S(1)} %get-tuple-element.112), channel_id=1, source_target_pairs={{0,16},{1,17},{2,18},{3,19},{4,20},{5,21},{6,22},{7,23},{8,24},{9,... | collective-permute-start | bytes 1179656 | tf_op jit(solution)/shard_map/ppermute | solution.py:324
  51.7 20.5 %collective-permute-start.38 = (bf16[8,96,256]{2,1,0:T(8,128)(2,1)S(1)}, bf16[8,96,256]{2,1,0:T(8,128)(2,1)S(1)}, u32[]{:S(2)}, u32[]{:S(2)}) collective-permute-start(bf16[8,96,256]{2,1,0:T(8,128)(2,1)S(1)} %get-tuple-element.113), channel_id=1, source_target_pairs={{0,24},{1,25},{2,26},{3,27},{4,28},{5,29},{6,30},{7,31},{8,16},{9,... | collective-permute-start | bytes 1179656 | tf_op jit(solution)/shard_map/ppermute | solution.py:324
  59.1 16.5 %collective-permute-start.22 = (bf16[4,48,2048]{2,1,0:T(8,128)(2,1)S(1)}, bf16[4,48,2048]{2,1,0:T(8,128)(2,1)S(1)}, u32[]{:S(2)}, u32[]{:S(2)}) collective-permute-start(bf16[4,48,2048]{2,1,0:T(8,128)(2,1)S(1)} %get-tuple-element.93), channel_id=1, source_target_pairs={{0,1},{1,0},{2,3},{3,2},{4,5},{5,4},{6,7},{7,6},{8,9},{9,8},{10,11... | collective-permute-start | bytes 2359304 | tf_op jit(solution)/shard_map/ppermute | solution.py:343
  75.5 3.8 %collective-permute-start.39 = (bf16[4,48,2048]{2,1,0:T(8,128)(2,1)S(1)}, bf16[4,48,2048]{2,1,0:T(8,128)(2,1)S(1)}, u32[]{:S(2)}, u32[]{:S(2)}) collective-permute-start(bf16[4,48,2048]{2,1,0:T(8,128)(2,1)S(1)} %get-tuple-element.115), channel_id=1, source_target_pairs={{0,1},{1,0},{2,3},{3,2},{4,5},{5,4},{6,7},{7,6},{8,9},{9,8},{10,11... | collective-permute-start | bytes 2359304 | tf_op jit(solution)/shard_map/ppermute | solution.py:343
  75.7 12.1 %collective-permute-start.23 = (bf16[96,2048]{1,0:T(8,128)(2,1)S(1)}, bf16[96,2048]{1,0:T(8,128)(2,1)S(1)}, u32[]{:S(2)}, u32[]{:S(2)}) collective-permute-start(bf16[96,2048]{1,0:T(8,128)(2,1)S(1)} %get-tuple-element.95), channel_id=1, source_target_pairs={{0,8},{1,9},{2,10},{3,11},{4,12},{5,13},{6,14},{7,15},{8,0},{9,1},... | collective-permute-start | bytes 1179656 | tf_op jit(solution)/shard_map/ppermute | solution.py:354
  77.2 20.4 %collective-permute-start.24 = (bf16[96,2048]{1,0:T(8,128)(2,1)S(1)}, bf16[96,2048]{1,0:T(8,128)(2,1)S(1)}, u32[]{:S(2)}, u32[]{:S(2)}) collective-permute-start(bf16[96,2048]{1,0:T(8,128)(2,1)S(1)} %get-tuple-element.96), channel_id=1, source_target_pairs={{0,16},{1,17},{2,18},{3,19},{4,20},{5,21},{6,22},{7,23},{8,24},{9,... | collective-permute-start | bytes 1179656 | tf_op jit(solution)/shard_map/ppermute | solution.py:354
  78.8 18.9 %collective-permute-start.25 = (bf16[96,2048]{1,0:T(8,128)(2,1)S(1)}, bf16[96,2048]{1,0:T(8,128)(2,1)S(1)}, u32[]{:S(2)}, u32[]{:S(2)}) collective-permute-start(bf16[96,2048]{1,0:T(8,128)(2,1)S(1)} %get-tuple-element.97), channel_id=1, source_target_pairs={{0,24},{1,25},{2,26},{3,27},{4,28},{5,29},{6,30},{7,31},{8,16},{9,... | collective-permute-start | bytes 1179656 | tf_op jit(solution)/shard_map/ppermute | solution.py:354
  79.4 21.1 %collective-permute-start.40 = (bf16[96,1024]{1,0:T(8,128)(2,1)S(1)}, bf16[96,1024]{1,0:T(8,128)(2,1)S(1)}, u32[]{:S(2)}, u32[]{:S(2)}) collective-permute-start(bf16[96,1024]{1,0:T(8,128)(2,1)S(1)} %get-tuple-element.117), channel_id=1, source_target_pairs={{0,8},{1,9},{2,10},{3,11},{4,12},{5,13},{6,14},{7,15},{8,0},{9,1},... | collective-permute-start | bytes 589832 | tf_op jit(solution)/shard_map/ppermute | solution.py:354
  80.9 25.2 %collective-permute-start.41 = (bf16[96,1024]{1,0:T(8,128)(2,1)S(1)}, bf16[96,1024]{1,0:T(8,128)(2,1)S(1)}, u32[]{:S(2)}, u32[]{:S(2)}) collective-permute-start(bf16[96,1024]{1,0:T(8,128)(2,1)S(1)} %get-tuple-element.118), channel_id=1, source_target_pairs={{0,16},{1,17},{2,18},{3,19},{4,20},{5,21},{6,22},{7,23},{8,24},{9,... | collective-permute-start | bytes 589832 | tf_op jit(solution)/shard_map/ppermute | solution.py:354
  87.7 19.6 %collective-permute-start.42 = (bf16[96,1024]{1,0:T(8,128)(2,1)S(1)}, bf16[96,1024]{1,0:T(8,128)(2,1)S(1)}, u32[]{:S(2)}, u32[]{:S(2)}) collective-permute-start(bf16[96,1024]{1,0:T(8,128)(2,1)S(1)} %get-tuple-element.119), channel_id=1, source_target_pairs={{0,24},{1,25},{2,26},{3,27},{4,28},{5,29},{6,30},{7,31},{8,16},{9,... | collective-permute-start | bytes 589832 | tf_op jit(solution)/shard_map/ppermute | solution.py:354
  97.7 13.2 %collective-permute-start.46 = (bf16[96,1024]{1,0:T(8,128)(2,1)S(1)}, bf16[96,1024]{1,0:T(8,128)(2,1)S(1)}, u32[]{:S(2)}, u32[]{:S(2)}) collective-permute-start(bf16[96,1024]{1,0:T(8,128)(2,1)S(1)} %get-tuple-element.128), channel_id=1, source_target_pairs={{0,8},{1,9},{2,10},{3,11},{4,12},{5,13},{6,14},{7,15},{8,0},{9,1},... | collective-permute-start | bytes 589832 | tf_op jit(solution)/shard_map/ppermute | solution.py:354
  97.7 15.2 %collective-permute-start.47 = (bf16[96,1024]{1,0:T(8,128)(2,1)S(1)}, bf16[96,1024]{1,0:T(8,128)(2,1)S(1)}, u32[]{:S(2)}, u32[]{:S(2)}) collective-permute-start(bf16[96,1024]{1,0:T(8,128)(2,1)S(1)} %get-tuple-element.129), channel_id=1, source_target_pairs={{0,16},{1,17},{2,18},{3,19},{4,20},{5,21},{6,22},{7,23},{8,24},{9,... | collective-permute-start | bytes 589832 | tf_op jit(solution)/shard_map/ppermute | solution.py:354
  100.4 21.0 %collective-permute-start.26 = (bf16[64,2048]{1,0:T(8,128)(2,1)S(1)}, bf16[64,2048]{1,0:T(8,128)(2,1)S(1)}, u32[]{:S(2)}, u32[]{:S(2)}) collective-permute-start(bf16[64,2048]{1,0:T(8,128)(2,1)S(1)} %get-tuple-element.102), channel_id=1, source_target_pairs={{2,0},{3,1},{4,6},{5,7},{10,8},{11,9},{12,14},{13,15},{18,16},{19,... | collective-permute-start | bytes 786440 | tf_op jit(solution)/shard_map/ppermute | solution.py:380
  106.1 16.1 %collective-permute-start.27 = (bf16[64,2048]{1,0:T(8,128)(2,1)S(1)}, bf16[64,2048]{1,0:T(8,128)(2,1)S(1)}, u32[]{:S(2)}, u32[]{:S(2)}) collective-permute-start(bf16[64,2048]{1,0:T(8,128)(2,1)S(1)} %get-tuple-element.103), channel_id=1, source_target_pairs={{4,0},{5,1},{2,6},{3,7},{12,8},{13,9},{10,14},{11,15},{20,16},{21,... | collective-permute-start | bytes 786440 | tf_op jit(solution)/shard_map/ppermute | solution.py:380
  107.4 18.5 %collective-permute-start.28 = (bf16[64,2048]{1,0:T(8,128)(2,1)S(1)}, bf16[64,2048]{1,0:T(8,128)(2,1)S(1)}, u32[]{:S(2)}, u32[]{:S(2)}) collective-permute-start(bf16[64,2048]{1,0:T(8,128)(2,1)S(1)} %get-tuple-element.104), channel_id=1, source_target_pairs={{6,0},{7,1},{0,6},{1,7},{14,8},{15,9},{8,14},{9,15},{22,16},{23,17... | collective-permute-start | bytes 786440 | tf_op jit(solution)/shard_map/ppermute | solution.py:380
  110.9 6.6 %collective-permute-start.48 = (bf16[96,1024]{1,0:T(8,128)(2,1)S(1)}, bf16[96,1024]{1,0:T(8,128)(2,1)S(1)}, u32[]{:S(2)}, u32[]{:S(2)}) collective-permute-start(bf16[96,1024]{1,0:T(8,128)(2,1)S(1)} %get-tuple-element.130), channel_id=1, source_target_pairs={{0,24},{1,25},{2,26},{3,27},{4,28},{5,29},{6,30},{7,31},{8,16},{9,... | collective-permute-start | bytes 589832 | tf_op jit(solution)/shard_map/ppermute | solution.py:354
  112.9 14.5 %collective-permute-start.43 = (bf16[64,1024]{1,0:T(8,128)(2,1)S(1)}, bf16[64,1024]{1,0:T(8,128)(2,1)S(1)}, u32[]{:S(2)}, u32[]{:S(2)}) collective-permute-start(bf16[64,1024]{1,0:T(8,128)(2,1)S(1)} %get-tuple-element.124), channel_id=1, source_target_pairs={{0,2},{1,3},{6,4},{7,5},{8,10},{9,11},{14,12},{15,13},{16,18},{17,... | collective-permute-start | bytes 393224 | tf_op jit(solution)/shard_map/ppermute | solution.py:380
  117.5 10.5 %collective-permute-start.44 = (bf16[64,1024]{1,0:T(8,128)(2,1)S(1)}, bf16[64,1024]{1,0:T(8,128)(2,1)S(1)}, u32[]{:S(2)}, u32[]{:S(2)}) collective-permute-start(bf16[64,1024]{1,0:T(8,128)(2,1)S(1)} %get-tuple-element.125), channel_id=1, source_target_pairs={{6,2},{7,3},{0,4},{1,5},{14,10},{15,11},{8,12},{9,13},{22,18},{23,... | collective-permute-start | bytes 393224 | tf_op jit(solution)/shard_map/ppermute | solution.py:380
  121.5 6.6 %collective-permute-start.45 = (bf16[64,1024]{1,0:T(8,128)(2,1)S(1)}, bf16[64,1024]{1,0:T(8,128)(2,1)S(1)}, u32[]{:S(2)}, u32[]{:S(2)}) collective-permute-start(bf16[64,1024]{1,0:T(8,128)(2,1)S(1)} %get-tuple-element.126), channel_id=1, source_target_pairs={{4,2},{5,3},{2,4},{3,5},{12,10},{13,11},{10,12},{11,13},{20,18},{2... | collective-permute-start | bytes 393224 | tf_op jit(solution)/shard_map/ppermute | solution.py:380
  122.2 6.2 %collective-permute-start.49 = (bf16[64,1024]{1,0:T(8,128)(2,1)S(1)}, bf16[64,1024]{1,0:T(8,128)(2,1)S(1)}, u32[]{:S(2)}, u32[]{:S(2)}) collective-permute-start(bf16[64,1024]{1,0:T(8,128)(2,1)S(1)} %get-tuple-element.132), channel_id=1, source_target_pairs={{0,2},{1,3},{6,4},{7,5},{8,10},{9,11},{14,12},{15,13},{16,18},{17,... | collective-permute-start | bytes 393224 | tf_op jit(solution)/shard_map/ppermute | solution.py:380
  125.9 4.0 %collective-permute-start.50 = (bf16[64,1024]{1,0:T(8,128)(2,1)S(1)}, bf16[64,1024]{1,0:T(8,128)(2,1)S(1)}, u32[]{:S(2)}, u32[]{:S(2)}) collective-permute-start(bf16[64,1024]{1,0:T(8,128)(2,1)S(1)} %get-tuple-element.133), channel_id=1, source_target_pairs={{6,2},{7,3},{0,4},{1,5},{14,10},{15,11},{8,12},{9,13},{22,18},{23,... | collective-permute-start | bytes 393224 | tf_op jit(solution)/shard_map/ppermute | solution.py:380
  (8 other events, 126.3 us)
